TPU v7x, 32 devices: a whole 2x2x4 slice. The times are simulated.
32 devices in a mesh: fs: 8 (over z, core), tp: 4 (over y, x).
Axes of the slice: x: 2, y: 2, z: 4, core: 2. Of those that a mesh axis runs over, the one named last changes fastest.
Arguments:
- tokens: bfloat16 [1024, 2048], P('fs'), may hold values from -6 to 6
- experts: int32 [1024, 4], P('fs'), may hold values from 0 to 7, all different within a row; in each aligned block of 128 rows (0 to 127, 128 to 255, ...) at most 96 rows name the same one
- routing: float32 [1024, 4], P('fs'), may hold values from 0.05 to 0.6
- norm_gain: float32 [2048], replicated, may hold values from 0.1 to 1.9
- gate_master: float32 [8, 2048, 2048], P(None, 'fs', 'tp'), may hold values from -0.625 to 0.625
- linear_master: float32 [8, 2048, 2048], P(None, 'fs', 'tp'), may hold values from -0.625 to 0.625
- down_weight: bfloat16 [8, 2048, 2048], P('fs', None, 'tp'), may hold values from -0.013671875 to 0.013671875
Outputs:
- gate_out: bfloat16 [8, 2048, 2048], P('fs', None, 'tp')
- linear_out: bfloat16 [8, 2048, 2048], P('fs', None, 'tp')
- expert_mix: bfloat16 [1024, 2048], P('fs', 'tp')
Inputs may be any that keep to these rules, and one draw needn't show every extreme that they name: Each row names 4 different experts; within the rows of one index of fs (aligned blocks of 128 rows) no expert is named by more than 96 rows, and in some blocks some expert is named by exactly 96; every expert is named somewhere.
All inputs are finite; a program needn't handle non-finite values.
Results may differ from a plain program's by a relative error of at most 0.023.
Values may be sent and summed in bfloat16 or wider, within the bound.
No kernel may reach another device: no remote copies, remote signals or barrier semaphores. Data moves between devices by JAX's collectives and lax.ppermute only.
A program may use at most 64 MiB of HBM per device.

v0:
```python
import jax
import jax.numpy as jnp
from jax import lax
from jax.sharding import PartitionSpec as P

clamp_limit = 7.0
gate_slope = 1.702


def on_device(tokens, experts, routing, norm_gain, gate_master, linear_master, down_weight):
    tok_count, top_count = experts.shape
    expert_count = gate_master.shape[0]
    width = tokens.shape[1]
    capacity = 3 * tok_count * top_count // (2 * expert_count)
    moved_gate, moved_linear = (
        lax.all_to_all(
            gate_master.astype(jnp.bfloat16), "fs", split_axis=0, concat_axis=1, tiled=True
        ).astype(gate_master.dtype),
        lax.all_to_all(
            linear_master.astype(jnp.bfloat16), "fs", split_axis=0, concat_axis=1, tiled=True
        ).astype(linear_master.dtype),
    )
    gate_out = (moved_gate * norm_gain[None, :, None]).astype(jnp.bfloat16)
    linear_out = (moved_linear * norm_gain[None, :, None]).astype(jnp.bfloat16)
    flat_ids = experts.reshape(-1)
    one_hot = (flat_ids[:, None] == jnp.arange(expert_count, dtype=jnp.int32)[None, :]).astype(
        jnp.int32
    )
    slot_rank = jnp.sum((jnp.cumsum(one_hot, axis=0) - one_hot) * one_hot, axis=1)
    slot_index = flat_ids * capacity + slot_rank
    owner = jnp.arange(tok_count * top_count, dtype=jnp.int32) // top_count
    slot_token = (
        jnp.full((expert_count * capacity,), tok_count, jnp.int32).at[slot_index].set(owner)
    )
    padded = jnp.concatenate([tokens, jnp.zeros((1, width), tokens.dtype)], axis=0)
    sender = padded[slot_token].reshape(expert_count, capacity, width)
    gate_local = gate_out[0]
    linear_local = linear_out[0]
    down_local = down_weight[0]
    item_rows = lax.all_to_all(sender, "fs", split_axis=0, concat_axis=0, tiled=True)
    flat_rows = item_rows.reshape(-1, width)
    pre_gate = jnp.dot(flat_rows, gate_local, preferred_element_type=jnp.float32)
    pre_linear = jnp.dot(flat_rows, linear_local, preferred_element_type=jnp.float32)
    clamped = jnp.minimum(pre_gate, clamp_limit)
    active = (
        clamped
        * jax.nn.sigmoid(gate_slope * clamped)
        * (jnp.clip(pre_linear, -clamp_limit, clamp_limit) + 1.0)
    ).astype(jnp.bfloat16)
    partial_value = lax.dot_general(
        active, down_local, (((1,), (1,)), ((), ())), preferred_element_type=jnp.float32
    ).reshape(item_rows.shape)
    results = partial_value.astype(jnp.bfloat16)
    summed = lax.psum_scatter(results, "tp", scatter_dimension=2, tiled=True).astype(jnp.float32)
    returned = lax.all_to_all(
        summed.astype(jnp.bfloat16), "fs", split_axis=0, concat_axis=0, tiled=True
    ).astype(summed.dtype)
    picked = returned.reshape(expert_count * capacity, -1)[slot_index].reshape(
        tok_count, top_count, -1
    )
    expert_mix = jnp.sum(routing[:, :, None] * picked, axis=1).astype(jnp.bfloat16)
    return (gate_out, linear_out, expert_mix)


def solution(mesh):
    placed = (
        P("fs", None),
        P("fs", None),
        P("fs", None),
        P(),
        P(None, "fs", "tp"),
        P(None, "fs", "tp"),
        P("fs", None, "tp"),
    )
    return jax.shard_map(
        on_device,
        mesh=mesh,
        in_specs=placed,
        out_specs=(P("fs", None, "tp"), P("fs", None, "tp"), P("fs", "tp")),
        check_vma=False,
    )
```

profile of v0, /device:TPU:0, one launch (start us, length us, event | category | flops | bytes accessed | tf_op | source)
XLA Modules:
  0.0 293.1 jit_solution(636927419273226423)
XLA Ops:
  7.2 3.9 %convert_element_type.149 = bf16[8,256,512]{2,1,0:T(8,128)(2,1)} convert(f32[8,256,512]{2,1,0:T(8,128)} %param.11) | non-fusion elementwise | flops 1048576 | bytes 6291456 | tf_op jit(solution)/shard_map/convert_element_type | solution.py:17
  11.1 6.4 %all-to-all-start = ((bf16[8,256,512]{2,1,0:T(8,128)(2,1)}), bf16[8,256,512]{2,1,0:T(8,128)(2,1)}, u32[]{:S(2)}, u32[]{:S(2)}) async-start(bf16[8,256,512]{2,1,0:T(8,128)(2,1)} %convert_element_type.149), calls=%async_computation | async-start | bytes 4194304 | tf_op jit(solution)/shard_map/all_to_all | solution.py:16
  17.5 3.8 %convert_element_type.153 = bf16[8,256,512]{2,1,0:T(8,128)(2,1)} convert(f32[8,256,512]{2,1,0:T(8,128)} %param.12) | non-fusion elementwise | flops 1048576 | bytes 6291456 | tf_op jit(solution)/shard_map/convert_element_type | solution.py:20
  21.2 45.4 %all-to-all-done = bf16[8,256,512]{2,1,0:T(8,128)(2,1)} async-done(((bf16[8,256,512]{2,1,0:T(8,128)(2,1)}), bf16[8,256,512]{2,1,0:T(8,128)(2,1)}, u32[]{:S(2)}, u32[]{:S(2)}) %all-to-all-start) | async-done | bytes 2097184 | tf_op jit(solution)/shard_map/all_to_all | solution.py:16
  66.6 4.4 %all-to-all-start.1 = ((bf16[8,256,512]{2,1,0:T(8,128)(2,1)}), bf16[8,256,512]{2,1,0:T(8,128)(2,1)}, u32[]{:S(2)}, u32[]{:S(2)}) async-start(bf16[8,256,512]{2,1,0:T(8,128)(2,1)} %convert_element_type.153), calls=%async_computation.1 | async-start | bytes 4194304 | tf_op jit(solution)/shard_map/all_to_all | solution.py:19
  71.0 0.1 copy.13
  71.1 0.1 eq.29
  71.2 0.1 eq.25
  71.3 0.1 copy.12
  71.4 0.1 mul.109
  71.5 1.1 reduce-window.6
  72.7 0.2 slice_reduce_fusion
  73.0 0.1 fusion.14
  73.1 2.4 scatter_custom_fusion
  75.6 4.2 %gather_fusion = bf16[768,2048]{1,0:T(8,128)(2,1)} fusion(bf16[129,2048]{1,0:T(8,128)(2,1)S(1)} %concatenate.3, s32[1024]{0:T(1024)S(1)} %pad_clamp_fusion.1), kind=kCustom, calls=%fused_computation | custom fusion | bytes 6294528 | tf_op jit(solution)/shard_map/gather | solution.py:36
  79.8 40.2 %all-to-all-done.1 = bf16[8,256,512]{2,1,0:T(8,128)(2,1)} async-done(((bf16[8,256,512]{2,1,0:T(8,128)(2,1)}), bf16[8,256,512]{2,1,0:T(8,128)(2,1)}, u32[]{:S(2)}, u32[]{:S(2)}) %all-to-all-start.1) | async-done | bytes 2097184 | tf_op jit(solution)/shard_map/all_to_all | solution.py:19
  120.0 4.5 %all-to-all-start.2 = ((bf16[8,96,2048]{2,1,0:T(8,128)(2,1)}), bf16[8,96,2048]{2,1,0:T(8,128)(2,1)}, u32[]{:S(2)}, u32[]{:S(2)}) async-start(bf16[8,96,2048]{2,1,0:T(8,128)(2,1)} %bitcast.47), calls=%async_computation.2 | async-start | bytes 6291456 | tf_op jit(solution)/shard_map/all_to_all | solution.py:40
  124.5 4.1 %convert_element_type.170 = f32[8,256,512]{2,1,0:T(8,128)} convert(bf16[8,256,512]{2,1,0:T(8,128)(2,1)} %all-to-all-done) | non-fusion elementwise | flops 1048576 | bytes 6291456 | tf_op jit(solution)/shard_map/convert_element_type | solution.py:18
  128.6 4.2 %convert_element_type.171 = f32[8,256,512]{2,1,0:T(8,128)} convert(bf16[8,256,512]{2,1,0:T(8,128)(2,1)} %all-to-all-done.1) | non-fusion elementwise | flops 1048576 | bytes 6291456 | tf_op jit(solution)/shard_map/convert_element_type | solution.py:21
  132.8 63.2 %all-to-all-done.2 = bf16[8,96,2048]{2,1,0:T(8,128)(2,1)} async-done(((bf16[8,96,2048]{2,1,0:T(8,128)(2,1)}), bf16[8,96,2048]{2,1,0:T(8,128)(2,1)}, u32[]{:S(2)}, u32[]{:S(2)}) %all-to-all-start.2) | async-done | bytes 3145760 | tf_op jit(solution)/shard_map/all_to_all | solution.py:40
  196.0 5.1 %fusion.3 = f32[768,512]{1,0:T(8,128)S(1)} fusion(bf16[768,2048]{1,0:T(8,128)(2,1)} %bitcast.7, f32[1,2048,1,1,1,1,512]{6,1,5,4,3,2,0:T(8,128)} %bitcast.43, f32[2048]{0:T(1024)S(1)} %copy-done.4), kind=kOutput, calls=%fused_computation.11 | convolution fusion | flops 1612709888 | bytes 8921088 | tf_op jit(solution)/shard_map/dot_general | solution.py:42
  201.2 4.1 %multiply_convert_fusion.2 = bf16[768,512]{1,0:T(8,128)(2,1)S(1)} fusion(f32[768,512]{1,0:T(8,128)S(1)} %fusion.3, bf16[768,2048]{1,0:T(8,128)(2,1)} %bitcast.7, f32[1,2048,1,1,1,1,512]{6,1,5,4,3,2,0:T(8,128)S(1)} %bitcast.46, f32[2048]{0:T(1024)S(1)} %copy-done.4), kind=kOutput, calls=%fused_computation.17 | convolution fusion | flops 1616642048 | bytes 9707520 | tf_op jit(solution)/shard_map/dot_general | solution.py:43
  205.3 3.6 %convolution_convert_fusion = bf16[8,96,2048]{2,1,0:T(8,128)(2,1)} fusion(bf16[8,96,512]{2,1,0:T(8,128)(2,1)S(1)} %bitcast.51, bf16[1,2048,512]{2,1,0:T(8,128)(2,1)S(1)} %copy-done), kind=kOutput, calls=%fused_computation.9 | convolution fusion | flops 1612185600 | bytes 6029312 | tf_op jit(solution)/shard_map/dot_general | solution.py:50
  209.0 43.0 %reduce-scatter.2.cloned.1.call-done = bf16[8,96,512]{2,1,0:T(8,128)(2,1)} async-done(((bf16[8,96,2048]{2,1,0:T(8,128)(2,1)}), bf16[8,96,512]{2,1,0:T(8,128)(2,1)}) %reduce-scatter.2.cloned.1.call-update) | async-done | bytes 786448 | tf_op jit(solution)/shard_map/reduce_scatter | solution.py:54
  251.9 4.6 %all-to-all-start.3 = ((bf16[8,96,512]{2,1,0:T(8,128)(2,1)}), bf16[8,96,512]{2,1,0:T(8,128)(2,1)S(1)}, u32[]{:S(2)}, u32[]{:S(2)}) async-start(bf16[8,96,512]{2,1,0:T(8,128)(2,1)} %reduce-scatter.2.cloned.1.call-done), calls=%async_computation.4 | async-start | bytes 1572864 | tf_op jit(solution)/shard_map/all_to_all | solution.py:55
  256.5 0.1 copy.11
  256.7 6.0 %fusion = (bf16[1,2048,512]{2,1,0:T(8,128)(2,1)}, bf16[1,2048,512]{2,1,0:T(8,128)(2,1)}) fusion(f32[2048]{0:T(1024)S(1)} %copy-done.4, f32[1,2048,512]{2,1,0:T(8,128)} %bitcast.45, f32[1,2048,512]{2,1,0:T(8,128)} %bitcast.44), kind=kLoop, calls=%fused_computation.4 | loop fusion | flops 4194304 | bytes 12591104 | tf_op jit(solution)/shard_map/convert_element_type | solution.py:24
  262.7 14.8 %all-to-all-done.3 = bf16[8,96,512]{2,1,0:T(8,128)(2,1)S(1)} async-done(((bf16[8,96,512]{2,1,0:T(8,128)(2,1)}), bf16[8,96,512]{2,1,0:T(8,128)(2,1)S(1)}, u32[]{:S(2)}, u32[]{:S(2)}) %all-to-all-start.3) | async-done | bytes 786464 | tf_op jit(solution)/shard_map/all_to_all | solution.py:55
  277.5 1.4 bitcast_convert_fusion
  278.9 3.4 %gather_fusion.1 = f32[512,512]{1,0:T(8,128)S(1)} fusion(f32[768,512]{1,0:T(8,128)} %bitcast_convert_fusion, s32[1024]{0:T(1024)S(1)} %pad_clamp_fusion), kind=kCustom, calls=%fused_computation.1 | custom fusion | bytes 2099200 | tf_op jit(solution)/shard_map/gather | solution.py:58
  282.3 1.3 reshape.249
  283.6 2.6 multiply_reduce_fusion
  (24 shorter events, 0.2 us)
Async XLA Ops:
  7.2 198.1 %copy-start = (bf16[1,2048,512]{2,1,0:T(8,128)(2,1)S(1)}, bf16[1,2048,512]{2,1,0:T(8,128)(2,1)}, u32[]{:S(2)}) copy-start(bf16[1,2048,512]{2,1,0:T(8,128)(2,1)} %param.13) | copy-start | bytes 6291460
  11.1 55.5 %all-to-all-start = ((bf16[8,256,512]{2,1,0:T(8,128)(2,1)}), bf16[8,256,512]{2,1,0:T(8,128)(2,1)}, u32[]{:S(2)}, u32[]{:S(2)}) async-start(bf16[8,256,512]{2,1,0:T(8,128)(2,1)} %convert_element_type.149), calls=%async_computation | async-start | bytes 4194304 | tf_op jit(solution)/shard_map/all_to_all | solution.py:16
  21.2 49.7 %copy-start.3 = (s32[128,4]{0,1:T(4,128)S(1)}, s32[128,4]{0,1:T(4,128)}, u32[]{:S(2)}) copy-start(s32[128,4]{0,1:T(4,128)} %param.8) | copy-start | bytes 6148
  21.2 51.7 %copy-start.2 = (bf16[128,2048]{1,0:T(8,128)(2,1)S(1)}, bf16[128,2048]{1,0:T(8,128)(2,1)}, u32[]{:S(2)}) copy-start(bf16[128,2048]{1,0:T(8,128)(2,1)} %param.7) | copy-start | bytes 1572868
  66.6 53.4 %all-to-all-start.1 = ((bf16[8,256,512]{2,1,0:T(8,128)(2,1)}), bf16[8,256,512]{2,1,0:T(8,128)(2,1)}, u32[]{:S(2)}, u32[]{:S(2)}) async-start(bf16[8,256,512]{2,1,0:T(8,128)(2,1)} %convert_element_type.153), calls=%async_computation.1 | async-start | bytes 4194304 | tf_op jit(solution)/shard_map/all_to_all | solution.py:19
  120.0 76.0 %all-to-all-start.2 = ((bf16[8,96,2048]{2,1,0:T(8,128)(2,1)}), bf16[8,96,2048]{2,1,0:T(8,128)(2,1)}, u32[]{:S(2)}, u32[]{:S(2)}) async-start(bf16[8,96,2048]{2,1,0:T(8,128)(2,1)} %bitcast.47), calls=%async_computation.2 | async-start | bytes 6291456 | tf_op jit(solution)/shard_map/all_to_all | solution.py:40
  124.5 127.4 %reduce-scatter.2.cloned.1.call-start = ((), (), s32[]{:S(2)}) async-start(), calls=%async_computation.5 | async-start | bytes 3932160 | tf_op jit(solution)/shard_map/reduce_scatter | solution.py:54
  128.6 67.4 %copy-start.4 = (f32[2048]{0:T(1024)S(1)}, f32[2048]{0:T(1024)}, u32[]{:S(2)}) copy-start(f32[2048]{0:T(1024)} %param.10) | copy-start | bytes 24580
  196.0 5.2 %copy-start.1 = (f32[8,256,512]{2,1,0:T(8,128)S(1)}, f32[8,256,512]{2,1,0:T(8,128)}, u32[]{:S(2)}) copy-start(f32[8,256,512]{2,1,0:T(8,128)} %convert_element_type.171) | copy-start | bytes 12582916
  208.9 47.6 %copy-start.5 = (f32[128,4]{0,1:T(4,128)S(1)}, f32[128,4]{0,1:T(4,128)}, u32[]{:S(2)}) copy-start(f32[128,4]{0,1:T(4,128)} %param.9) | copy-start | bytes 6148
  251.9 25.6 %all-to-all-start.3 = ((bf16[8,96,512]{2,1,0:T(8,128)(2,1)}), bf16[8,96,512]{2,1,0:T(8,128)(2,1)S(1)}, u32[]{:S(2)}, u32[]{:S(2)}) async-start(bf16[8,96,512]{2,1,0:T(8,128)(2,1)} %reduce-scatter.2.cloned.1.call-done), calls=%async_computation.4 | async-start | bytes 1572864 | tf_op jit(solution)/shard_map/all_to_all | solution.py:55
Sparse Core Ops, SparseCore 0:
  209.1 42.8 reduce-scatter.1
where the time goes:
time: 294 us; the launch traced here: 293 us
  waiting for transfers between devices  207 us (70%)
  other arithmetic  27.3 us (9%)
  starting transfers between devices  19.9 us (7%)
  between operations  14.2 us (5%)
  matrix products  12.9 us (4%)
  local copies, waits for them, and re-layouts  12.4 us (4%)
    all_to_all x1, waiting for transfers between devices, on_device(): lax.all_to_all(sender, 'fs', split_axis=0, concat_axis=0, tiled=True)  63.2 us
    all_to_all x1, waiting for transfers between devices, on_device(): lax.all_to_all(gate_master.astype(jnp.bfloat16), 'fs', split_axis=0, conc...  45.4 us
    reduce_scatter x1, waiting for transfers between devices, on_device(): lax.psum_scatter(results, 'tp', scatter_dimension=2, tiled=True)  43 us
    all_to_all x1, waiting for transfers between devices, on_device(): lax.all_to_all(linear_master.astype(jnp.bfloat16), 'fs', split_axis=0, co...  40.2 us
    all_to_all x1, waiting for transfers between devices, on_device(): lax.all_to_all(summed.astype(jnp.bfloat16), 'fs', split_axis=0, concat_ax...  14.8 us
    convert_element_type x2, other arithmetic, on_device(): moved_gate, moved_linear = (lax.all_to_all(gate_master.astype(jnp.bfloat1...  8.24 us
    all_to_all x1, starting transfers between devices, on_device(): lax.all_to_all(gate_master.astype(jnp.bfloat16), 'fs', split_axis=0, conc...  6.35 us
    convert_element_type x1, other arithmetic, on_device(): linear_out = (moved_linear * norm_gain[None, :, None]).astype(jnp.bfloat16)  6 us
  transfers between devices with their start and end apart: 5, of which 5 were waited for; matrix products, arithmetic and copies ran while one was open for 9% of the time, Pallas kernels for 0%

commit v1 on v0

v1 whole, which is shorter than its diff:
```python
import jax
import jax.numpy as jnp
from jax import lax
from jax.experimental import pallas as pl
from jax.experimental.pallas import tpu as pltpu
from jax.sharding import PartitionSpec as P

clamp_limit = 7.0
gate_slope = 1.702
lanes = 128


HBM = pl.BlockSpec(memory_space=pl.ANY)
VMEM = pl.BlockSpec(memory_space=pltpu.VMEM)
SMEM = pl.BlockSpec(memory_space=pltpu.SMEM)


def swap(value, axis, size, step):
    return lax.ppermute(value, axis, [(i, i ^ step) for i in range(size)])


def chunk_widths(hidden):
    count = hidden // lanes
    if count >= 3:
        return [hidden - 2 * lanes, lanes, lanes]
    return [lanes] * count


def grant(used):
    return pltpu.CompilerParams(vmem_limit_bytes=min(used + (8 << 20), 60 << 20))


def cost(flops, moved):
    return pl.CostEstimate(flops=flops, bytes_accessed=moved, transcendentals=0)


def convert(place, gain_col, gate_master, linear_master, widths):
    experts, rows, hidden = gate_master.shape
    kinds = len(widths)

    def kernel(place_ref, gain_ref, gate_ref, linear_ref, *refs):
        outs = refs[: kinds * experts]
        gate_buf, linear_buf = refs[kinds * experts : kinds * experts + 2]
        bufs = refs[kinds * experts + 2 : kinds * experts + 2 + kinds]
        in_sem, out_sem = refs[-2:]
        me = place_ref[0]
        loads = []
        for k in range(experts):
            pair = [
                pltpu.make_async_copy(gate_ref.at[me ^ k], gate_buf.at[k], in_sem.at[0, k]),
                pltpu.make_async_copy(linear_ref.at[me ^ k], linear_buf.at[k], in_sem.at[1, k]),
            ]
            order = pair
            for copy in order:
                copy.start()
            loads.append(pair)
        gain = gain_ref[...]
        stores = []
        for k in range(experts):
            for copy in loads[k]:
                copy.wait()
            offset = 0
            for c, width in enumerate(widths):
                span = slice(offset, offset + width)
                bufs[c][k, :, :width] = (gate_buf[k, :, span] * gain).astype(jnp.bfloat16)
                bufs[c][k, :, width:] = (linear_buf[k, :, span] * gain).astype(jnp.bfloat16)
                offset += width
                copy = pltpu.make_async_copy(bufs[c].at[k], outs[c * experts + k], out_sem.at[c, k])
                copy.start()
                stores.append(copy)
        for copy in stores:
            copy.wait()

    outs = pl.pallas_call(
        kernel,
        out_shape=[
            jax.ShapeDtypeStruct((rows, 2 * width), jnp.bfloat16) for width in widths for _ in range(experts)
        ],
        in_specs=[SMEM, VMEM, HBM, HBM],
        out_specs=[HBM] * (kinds * experts),
        scratch_shapes=[
            pltpu.VMEM((experts, rows, hidden), jnp.float32),
            pltpu.VMEM((experts, rows, hidden), jnp.float32),
            *[pltpu.VMEM((experts, rows, 2 * width), jnp.bfloat16) for width in widths],
            pltpu.SemaphoreType.DMA((2, experts)),
            pltpu.SemaphoreType.DMA((kinds, experts)),
        ],
        cost_estimate=cost(4 * experts * rows * hidden, 12 * experts * rows * hidden),
        name="convert",
    )(place, gain_col, gate_master, linear_master)
    return [outs[c * experts : (c + 1) * experts] for c in range(kinds)]


def activate(place, halves, pieces, built, offset, hidden):
    count = len(pieces)
    rows, width = pieces[0].shape[0], pieces[0].shape[1] // 2
    half, depth = halves[0].shape
    total = 2 * half
    block = min(512, half)

    def kernel(place_ref, xa_ref, xb_ref, *refs):
        piece_refs = refs[:count]
        active_ref, gate_ref, linear_ref, w_buf, o_sem = refs[count + len(built) :]
        me = place_ref[0]
        for k in range(count):
            row = pl.multiple_of((me ^ k) * rows, rows)
            w_buf[pl.ds(row, rows), :] = piece_refs[k][...]
        out_copies = [
            pltpu.make_async_copy(
                w_buf.at[:, pl.ds(s * width, width)], ref.at[:, pl.ds(offset, width)], o_sem.at[s]
            )
            for s, ref in enumerate((gate_ref, linear_ref))
        ]
        for copy in out_copies:
            copy.start()
        for h, x_ref in enumerate((xa_ref, xb_ref)):
            for n in range(half // block):
                pre = jnp.dot(
                    x_ref[pl.ds(n * block, block), :], w_buf[...], preferred_element_type=jnp.float32
                )
                clamped = jnp.minimum(pre[:, :width], clamp_limit)
                linear = jnp.clip(pre[:, width:], -clamp_limit, clamp_limit) + 1.0
                active_ref[pl.ds(h * half + n * block, block), :] = (
                    clamped * jax.nn.sigmoid(gate_slope * clamped) * linear
                ).astype(jnp.bfloat16)
        for copy in out_copies:
            copy.wait()

    out = jax.ShapeDtypeStruct((count * rows, hidden), jnp.bfloat16)
    return pl.pallas_call(
        kernel,
        out_shape=[jax.ShapeDtypeStruct((total, width), jnp.bfloat16), out, out],
        in_specs=[SMEM, VMEM, VMEM] + [VMEM] * count + [HBM] * len(built),
        out_specs=[VMEM, HBM, HBM],
        input_output_aliases={3 + count + n: 1 + n for n in range(len(built))},
        scratch_shapes=[
            pltpu.VMEM((count * rows, 2 * width), jnp.bfloat16),
            pltpu.SemaphoreType.DMA((2,)),
        ],
        compiler_params=grant(total * depth * 2 + 4 * count * rows * width * 2 + 2 * total * width * 6),
        cost_estimate=cost(4 * total * depth * width, 2 * total * depth),
        name="activate",
    )(place, *halves, *pieces, *built)


def assemble(place, shares):
    groups, sub, width = shares[0].shape
    parts = len(shares)

    def kernel(place_ref, *refs):
        for q in range(parts):
            row = pl.multiple_of((place_ref[1] ^ q) * sub, sub)
            for g in range(groups):
                refs[-1][g, pl.ds(row, sub), :] = refs[q][g]

    return pl.pallas_call(
        kernel,
        out_shape=jax.ShapeDtypeStruct((groups, parts * sub, width), shares[0].dtype),
        in_specs=[SMEM] + [VMEM] * parts,
        out_specs=VMEM,
        compiler_params=grant(4 * groups * parts * sub * width),
        cost_estimate=cost(groups * parts * sub * width, 4 * groups * parts * sub * width),
        name="assemble",
    )(place, *shares)


def project(actives, downs, offsets, running, scale):
    count, chunks = len(downs), len(actives)
    total = actives[0][0].shape[0]
    features = downs[0].shape[0]
    widths = [group[0].shape[1] for group in actives]
    block = min(256, total)
    blocks = total // block
    extra = ([running] if running is not None else []) + ([scale] if scale is not None else [])

    def kernel(*refs):
        active_refs = [refs[c * count : (c + 1) * count] for c in range(chunks)]
        down_refs = refs[chunks * count : (chunks + 1) * count]
        others = refs[(chunks + 1) * count :]
        sides = [
            jnp.concatenate([d[:, o : o + w] for d in down_refs], axis=1) for o, w in zip(offsets, widths)
        ]
        for n in range(blocks):
            span = slice(n * block, (n + 1) * block)
            acc = others[0][span, :] if running is not None else None
            for c in range(chunks):
                left = jnp.concatenate([a[span, :] for a in active_refs[c]], axis=1)
                part = lax.dot_general(
                    left, sides[c], (((1,), (1,)), ((), ())), preferred_element_type=jnp.float32
                )
                acc = part if acc is None else acc + part
            if scale is None:
                others[-1][span, :] = acc
            else:
                acc = acc * others[len(extra) - 1][span, :]
                if n < blocks // 2:
                    others[-2][span, :] = acc
                else:
                    others[-1][slice(n * block - total // 2, (n + 1) * block - total // 2), :] = acc.astype(
                        jnp.bfloat16
                    )

    if scale is None:
        shapes = jax.ShapeDtypeStruct((total, features), jnp.float32)
        specs = VMEM
    else:
        shapes = [
            jax.ShapeDtypeStruct((total // 2, features), jnp.float32),
            jax.ShapeDtypeStruct((total // 2, features), jnp.bfloat16),
        ]
        specs = [VMEM, VMEM]
    return pl.pallas_call(
        kernel,
        out_shape=shapes,
        in_specs=[VMEM] * ((chunks + 1) * count + len(extra)),
        out_specs=specs,
        compiler_params=grant(
            2 * count * total * sum(widths) + 4 * features * sum(d.shape[1] for d in downs) + 12 * total * features
        ),
        cost_estimate=cost(2 * total * features * count * sum(widths), 4 * total * features),
        name="project",
    )(*[a for group in actives for a in group], *downs, *extra)


def combine(kept, arrived, groups):
    total, features = kept.shape
    each = total // groups

    def kernel(kept_ref, arrived_ref, *outs):
        for g in range(groups):
            span = slice(g * each, (g + 1) * each)
            value = kept_ref[span, :] + arrived_ref[span, :].astype(jnp.float32)
            outs[g][...] = value.astype(outs[g].dtype)

    return pl.pallas_call(
        kernel,
        out_shape=[
            jax.ShapeDtypeStruct((each, features), jnp.bfloat16 if g else jnp.float32) for g in range(groups)
        ],
        in_specs=[VMEM, VMEM],
        out_specs=[VMEM] * groups,
        compiler_params=grant(12 * total * features),
        cost_estimate=cost(total * features, 8 * total * features),
        name="combine",
    )(kept, arrived)


def solution(mesh):
    n_fs, n_tp = mesh.shape["fs"], mesh.shape["tp"]
    n_z = n_fs // 2

    def on_device(tokens, experts, routing, norm_gain, gate_master, linear_master, down_weight):
        tok_count, width = tokens.shape
        expert_count, rows, hidden = gate_master.shape
        sub = tok_count // n_tp
        features = width // n_tp
        i, j = lax.axis_index("fs"), lax.axis_index("tp")
        place = jnp.stack([i, j]).astype(jnp.int32)

        share = lax.dynamic_slice_in_dim(tokens, j * sub, sub, 0)
        shares = jnp.stack([share] + [swap(share, "fs", n_fs, 2 * k) for k in range(1, n_z)])
        near = assemble(place, [shares] + [swap(shares, "tp", n_tp, q) for q in range(1, n_tp)])
        near = near.reshape(n_z * tok_count, width)
        far = swap(near, "fs", n_fs, 1)

        down_blocks = down_weight.reshape(n_tp, features, hidden)
        picked = [lax.dynamic_index_in_dim(down_blocks, j ^ q, 0, keepdims=False) for q in range(n_tp)]
        downs = [picked[0]] + [swap(picked[q], "tp", n_tp, q) for q in range(1, n_tp)]

        chosen = experts[:, :, None] == jnp.arange(expert_count, dtype=jnp.int32)[None, None, :]
        mixing = jnp.sum(jnp.where(chosen, routing[:, :, None], 0.0), axis=1).T
        mixing = jnp.stack([mixing] + [swap(mixing, "fs", n_fs, 2 * k) for k in range(1, n_z)])
        mixing = jnp.stack([mixing, swap(mixing, "fs", n_fs, 1)])
        scale = lax.dynamic_index_in_dim(mixing, i, 2, keepdims=False).reshape(-1, 1)

        widths = chunk_widths(hidden)
        offsets = [sum(widths[:c]) for c in range(len(widths))]
        gain_col = lax.dynamic_slice_in_dim(norm_gain, i * rows, rows, 0).reshape(rows, 1)
        pieces = convert(place, gain_col, gate_master, linear_master, widths)
        arrived = [[group[0]] + [swap(group[k], "fs", n_fs, k) for k in range(1, n_fs)] for group in pieces]

        built = []
        actives = []
        running = None
        for c in range(len(widths)):
            active, *built = activate(place, [near, far], arrived[c], built, offsets[c], hidden)
            actives.append([active] + [swap(active, "tp", n_tp, q) for q in range(1, n_tp)])

        if len(widths) > 1:
            running = project(actives[:-1], downs, offsets[:-1], None, None)
        kept, sent = project(actives[-1:], downs, offsets[-1:], running, scale)
        own, *others = combine(kept, swap(sent, "fs", n_fs, 1), n_z)
        total = own
        for k, other in enumerate(others, 1):
            total = total + swap(other, "fs", n_fs, 2 * k).astype(jnp.float32)
        return built[0][None], built[1][None], total.astype(jnp.bfloat16)

    placed = (
        P("fs", None),
        P("fs", None),
        P("fs", None),
        P(),
        P(None, "fs", "tp"),
        P(None, "fs", "tp"),
        P("fs", None, "tp"),
    )
    return jax.shard_map(
        on_device,
        mesh=mesh,
        in_specs=placed,
        out_specs=(P("fs", None, "tp"), P("fs", None, "tp"), P("fs", "tp")),
        check_vma=False,
    )
```

time: 294 us -> 249 us (0.85)
  waiting for transfers between devices: 207 us -> 126 us
  starting transfers between devices: 19.9 us -> 59.6 us
  other arithmetic: 27.3 us -> 1.48 us
  Pallas kernels: 0 us -> 25.4 us
  local copies, waits for them, and re-layouts: 12.4 us -> 35.5 us
  between operations: 14.2 us -> 1.11 us
  matrix products: 12.9 us -> 0 us
    all_to_all x4 -> x0, waiting for transfers between devices: 164 us -> none  [the longest x1 63.2 us: on_device(): lax.all_to_all(sender, 'fs', split_axis=0, concat_axis=0, tiled=True)]
    ppermute x0 -> x48, waiting for transfers between devices: none -> 126 us  [swap(): return lax.ppermute(value, axis, [(i, i ^ step) for i in range(size)])]
    ppermute x0 -> x48, starting transfers between devices: none -> 59.6 us  [swap(): return lax.ppermute(value, axis, [(i, i ^ step) for i in range(size)])]
    reduce_scatter x1 -> x0, waiting for transfers between devices: 43 us -> none  [on_device(): lax.psum_scatter(results, 'tp', scatter_dimension=2, tiled=True)]
    unnamed x14 -> x124, local copies, waits for them, and re-layouts: 0.25 us -> 31.9 us
    pallas_call x0 -> x8, Pallas kernels: none -> 25.4 us  [the longest x3 12.7 us: activate(): pl.pallas_call(kernel, out_shape=[jax.ShapeDtypeStruct((total, width), jn...]
    convert_element_type x6 -> x1, other arithmetic: 21.9 us -> 0.72 us  [on_device(): return (built[0][None], built[1][None], total.astype(jnp.bfloat16))]
    all_to_all x4 -> x0, starting transfers between devices: 19.8 us -> none  [the longest x1 6.35 us: on_device(): lax.all_to_all(gate_master.astype(jnp.bfloat16), 'fs', split_axis=0, conc...]
  transfers between devices with their start and end apart: 5 -> 48, of which waited for: 5 -> 19; matrix products, arithmetic and copies ran while one was open for 9% -> 2% of each run, Pallas kernels for 0% -> 9%
where the time goes in v1:
time: 249 us
  waiting for transfers between devices  126 us (51%)
  starting transfers between devices  59.6 us (24%)
  local copies, waits for them, and re-layouts  35.5 us (14%)
  Pallas kernels  25.4 us (10%)
    ppermute x48, waiting for transfers between devices, swap(): return lax.ppermute(value, axis, [(i, i ^ step) for i in range(size)])  126 us
    ppermute x48, starting transfers between devices, swap(): return lax.ppermute(value, axis, [(i, i ^ step) for i in range(size)])  59.6 us
    unnamed x124, local copies, waits for them, and re-layouts  31.9 us
    pallas_call x3, Pallas kernels, activate(): pl.pallas_call(kernel, out_shape=[jax.ShapeDtypeStruct((total, width), jn...  12.7 us
    pallas_call x1, Pallas kernels, convert(): pl.pallas_call(kernel, out_shape=[jax.ShapeDtypeStruct((rows, 2 * width),...  6.42 us
    pallas_call x2, Pallas kernels, project(): pl.pallas_call(kernel, out_shape=shapes, in_specs=[VMEM] * ((chunks + 1)...  5.52 us
  transfers between devices with their start and end apart: 48, of which 19 were waited for; matrix products, arithmetic and copies ran while one was open for 2% of the time, Pallas kernels for 9%

profile of v1, /device:TPU:0, one launch (start us, length us, event | category | flops | bytes accessed | tf_op | source)
XLA Modules:
  0.0 248.7 jit_solution(8649363891028954763)
XLA Ops:
  1.7 5.1 %collective-permute-start.2 = (bf16[32,2048]{1,0:T(8,128)(2,1)S(1)}, bf16[32,2048]{1,0:T(8,128)(2,1)S(1)}, u32[]{:S(2)}, u32[]{:S(2)}) collective-permute-start(bf16[32,2048]{1,0:T(8,128)(2,1)S(1)} %constant_dynamic-slice_fusion), channel_id=1, source_target_pairs={{0,24},{4,28},{8,16},{12,20},{16,8},{20,12},{24,0},{28,4},{1,25},{... | collective-permute-start | bytes 393224 | tf_op jit(solution)/shard_map/ppermute | solution.py:19
  7.5 3.8 %collective-permute-done.2 = bf16[32,2048]{1,0:T(8,128)(2,1)S(1)} collective-permute-done((bf16[32,2048]{1,0:T(8,128)(2,1)S(1)}, bf16[32,2048]{1,0:T(8,128)(2,1)S(1)}, u32[]{:S(2)}, u32[]{:S(2)}) %collective-permute-start.2) | collective-permute-done | bytes 131104 | tf_op jit(solution)/shard_map/ppermute | solution.py:19
  11.3 6.6 %collective-permute-done.1 = bf16[32,2048]{1,0:T(8,128)(2,1)S(1)} collective-permute-done((bf16[32,2048]{1,0:T(8,128)(2,1)S(1)}, bf16[32,2048]{1,0:T(8,128)(2,1)S(1)}, u32[]{:S(2)}, u32[]{:S(2)}) %collective-permute-start.1) | collective-permute-done | bytes 131104 | tf_op jit(solution)/shard_map/ppermute | solution.py:19
  21.6 11.2 %collective-permute-done.3.refs_1_ = bf16[4,32,2048]{2,1,0:T(8,128)(2,1)S(1)} collective-permute-done((bf16[4,32,2048]{2,1,0:T(8,128)(2,1)S(1)}, bf16[4,32,2048]{2,1,0:T(8,128)(2,1)S(1)}, u32[]{:S(2)}, u32[]{:S(2)}) %collective-permute-start.3) | collective-permute-done | bytes 524320 | tf_op jit(solution)/shard_map/ppermute | solution.py:19
  33.6 9.9 %collective-permute-done.4.refs_2_ = bf16[4,32,2048]{2,1,0:T(8,128)(2,1)S(1)} collective-permute-done((bf16[4,32,2048]{2,1,0:T(8,128)(2,1)S(1)}, bf16[4,32,2048]{2,1,0:T(8,128)(2,1)S(1)}, u32[]{:S(2)}, u32[]{:S(2)}) %collective-permute-start.4) | collective-permute-done | bytes 524320 | tf_op jit(solution)/shard_map/ppermute | solution.py:19
  49.5 2.4 collective-permute-start.42
  51.9 2.1 collective-permute-start.40
  55.6 6.4 %convert.1 = (bf16[256,512]{1,0:T(8,128)(2,1)}, bf16[256,512]{1,0:T(8,128)(2,1)}, bf16[256,512]{1,0:T(8,128)(2,1)}, bf16[256,512]{1,0:T(8,128)(2,1)}, bf16[256,5...) custom-call(s32[2]{0:T(128)} %copy-done.48, ...), custom_call_target="tpu_custom_call" | custom-call | flops 4194304 | bytes 12582912 | tf_op jit(solution)/shard_map/convert/pallas_call | solution.py:74
  65.5 1.9 collective-permute-start.10
  69.9 2.8 %collective-permute-done.9.refs_3_ = bf16[256,256]{1,0:T(8,128)(2,1)S(1)} collective-permute-done((bf16[256,256]{1,0:T(8,128)(2,1)}, bf16[256,256]{1,0:T(8,128)(2,1)S(1)}, u32[]{:S(2)}, u32[]{:S(2)}) %collective-permute-start.9) | collective-permute-done | bytes 131104 | tf_op jit(solution)/shard_map/ppermute | solution.py:19
  73.5 4.9 %collective-permute-done.10.refs_4_ = bf16[256,256]{1,0:T(8,128)(2,1)S(1)} collective-permute-done((bf16[256,256]{1,0:T(8,128)(2,1)}, bf16[256,256]{1,0:T(8,128)(2,1)S(1)}, u32[]{:S(2)}, u32[]{:S(2)}) %collective-permute-start.10) | collective-permute-done | bytes 131104 | tf_op jit(solution)/shard_map/ppermute | solution.py:19
  81.6 2.5 collective-permute-start.18
  84.7 2.3 collective-permute-start.19
  87.7 8.6 %collective-permute-done.17.refs_4_ = bf16[256,256]{1,0:T(8,128)(2,1)S(1)} collective-permute-done((bf16[256,256]{1,0:T(8,128)(2,1)}, bf16[256,256]{1,0:T(8,128)(2,1)S(1)}, u32[]{:S(2)}, u32[]{:S(2)}) %collective-permute-start.17) | collective-permute-done | bytes 131104 | tf_op jit(solution)/shard_map/ppermute | solution.py:19
  101.8 11.4 %collective-permute-done.20.refs_7_ = bf16[256,256]{1,0:T(8,128)(2,1)S(1)} collective-permute-done((bf16[256,256]{1,0:T(8,128)(2,1)}, bf16[256,256]{1,0:T(8,128)(2,1)S(1)}, u32[]{:S(2)}, u32[]{:S(2)}) %collective-permute-start.20) | collective-permute-done | bytes 131104 | tf_op jit(solution)/shard_map/ppermute | solution.py:19
  113.8 2.7 %collective-permute-start.25 = (bf16[256,512]{1,0:T(8,128)(2,1)}, bf16[256,512]{1,0:T(8,128)(2,1)}, u32[]{:S(2)}, u32[]{:S(2)}) collective-permute-start(bf16[256,512]{1,0:T(8,128)(2,1)} %get-tuple-element.63), channel_id=1, source_target_pairs={{0,20},{4,16},{8,28},{12,24},{16,4},{20,0},{24,12},{28,8},{1,21},{... | collective-permute-start | bytes 786440 | tf_op jit(solution)/shard_map/ppermute | solution.py:19
  117.2 1.8 collective-permute-start.26
  123.2 22.0 %collective-permute-done.24.refs_4_ = bf16[256,512]{1,0:T(8,128)(2,1)} collective-permute-done((bf16[256,512]{1,0:T(8,128)(2,1)}, bf16[256,512]{1,0:T(8,128)(2,1)}, u32[]{:S(2)}, u32[]{:S(2)}) %collective-permute-start.24) | collective-permute-done | bytes 262176 | tf_op jit(solution)/shard_map/ppermute | solution.py:19
  145.7 5.1 %collective-permute-done.25.refs_5_ = bf16[256,512]{1,0:T(8,128)(2,1)} collective-permute-done((bf16[256,512]{1,0:T(8,128)(2,1)}, bf16[256,512]{1,0:T(8,128)(2,1)}, u32[]{:S(2)}, u32[]{:S(2)}) %collective-permute-start.25) | collective-permute-done | bytes 262176 | tf_op jit(solution)/shard_map/ppermute | solution.py:19
  152.3 2.2 collective-permute-start.12
  155.8 5.1 %activate.3 = (bf16[1024,256]{1,0:T(8,128)(2,1)}, bf16[2048,512]{1,0:T(8,128)(2,1)}, bf16[2048,512]{1,0:T(8,128)(2,1)}) custom-call(s32[2]{0:T(128)S(1)} %copy-done.49, bf16[512,2048]{1,0:T(8,128)(2,1)S(1)} %bitcast.31, bf16[512,2048]{1,0:T(8,128)(2,1)} %collective-permute-done.6.xb_ref, bf16[256,512]{1,0:T(8,128)(2,1)S(1)} %copy-done.50, ...), custom_call_target="tpu_custom_call" | custom-call | flops 2147483648 | bytes 4194304 | tf_op jit(solution)/shard_map/activate/pallas_call | solution.py:130
  161.0 3.0 %activate.4 = (bf16[1024,128]{1,0:T(8,128)(2,1)S(1)}, bf16[2048,512]{1,0:T(8,128)(2,1)}, bf16[2048,512]{1,0:T(8,128)(2,1)}) custom-call(s32[2]{0:T(128)S(1)} %copy-done.49, bf16[512,2048]{1,0:T(8,128)(2,1)S(1)} %bitcast.32, bf16[512,2048]{1,0:T(8,128)(2,1)} %collective-permute-done.6.xb_ref, ...), custom_call_target="tpu_custom_call", output_to_operand_aliasing={{1}: (11, {}), {2}: (12, {})} | custom-call | flops 1073741824 | bytes 4194304 | tf_op jit(solution)/shard_map/activate/pallas_call | solution.py:130
  169.8 7.0 %collective-permute-done.32.refs_10_.refs_6_ = bf16[512,512]{1,0:T(8,128)(2,1)S(1)} collective-permute-done((bf16[512,512]{1,0:T(8,128)(2,1)S(1)}, bf16[512,512]{1,0:T(8,128)(2,1)S(1)}, u32[]{:S(2)}, u32[]{:S(2)}) %collective-permute-start.32) | collective-permute-done | bytes 524320 | tf_op jit(solution)/shard_map/ppermute | solution.py:19
  181.1 2.5 %collective-permute-start.39 = (bf16[1024,128]{1,0:T(8,128)(2,1)S(1)}, bf16[1024,128]{1,0:T(8,128)(2,1)}, u32[]{:S(2)}, u32[]{:S(2)}) collective-permute-start(bf16[1024,128]{1,0:T(8,128)(2,1)S(1)} %get-tuple-element.74.refs_4_), channel_id=1, source_target_pairs={{0,3},{1,2},{2,1},{3,0},{4,7},{5,6},{6,5},{7,4},{8,11},{9,10},{10,... | collective-permute-start | bytes 786440 | tf_op jit(solution)/shard_map/ppermute | solution.py:19
  190.0 4.5 %activate.5 = (bf16[1024,128]{1,0:T(8,128)(2,1)}, bf16[2048,512]{1,0:T(8,128)(2,1)}, bf16[2048,512]{1,0:T(8,128)(2,1)}) custom-call(s32[2]{0:T(128)S(1)} %copy-done.49, bf16[512,2048]{1,0:T(8,128)(2,1)S(1)} %bitcast.33, bf16[512,2048]{1,0:T(8,128)(2,1)} %collective-permute-done.6.xb_ref, ...), custom_call_target="tpu_custom_call", output_to_operand_aliasing={{1}: (11, {}), {2}: (12, {})} | custom-call | flops 1073741824 | bytes 4194304 | tf_op jit(solution)/shard_map/activate/pallas_call | solution.py:130
  194.5 15.3 %collective-permute-done.38.refs_6_ = bf16[1024,128]{1,0:T(8,128)(2,1)} collective-permute-done((bf16[1024,128]{1,0:T(8,128)(2,1)S(1)}, bf16[1024,128]{1,0:T(8,128)(2,1)}, u32[]{:S(2)}, u32[]{:S(2)}) %collective-permute-start.38) | collective-permute-done | bytes 262176 | tf_op jit(solution)/shard_map/ppermute | solution.py:19
  217.6 3.6 %project.2.refs_8_ = f32[1024,512]{1,0:T(8,128)S(1)} custom-call(bf16[1024,256]{1,0:T(8,128)(2,1)} %get-tuple-element.73.refs_0_, bf16[1024,256]{1,0:T(8,128)(2,1)} %collective-permute-done.34.refs_1_, bf16[1024,256]{1,0:T(8,128)(2,1)} %collective-permute-done.35.refs_2_, bf16[1024,256]{1,0:T(8,128)(2,1)} %collective-permute-done.36.refs_3_, ...), custom_call_target="tpu_custom_call" | custom-call | flops 1610612736 | bytes 2097152 | tf_op jit(solution)/shard_map/project/pallas_call | solution.py:212
  224.1 1.9 project.3
  226.2 1.9 collective-permute-done.44.arrived_ref
  228.1 2.2 collective-permute-start.47
  230.4 8.5 %collective-permute-start.46 = (bf16[128,512]{1,0:T(8,128)(2,1)S(1)}, bf16[128,512]{1,0:T(8,128)(2,1)S(1)}, u32[]{:S(2)}, u32[]{:S(2)}) collective-permute-start(bf16[128,512]{1,0:T(8,128)(2,1)S(1)} %get-tuple-element.79), channel_id=1, source_target_pairs={{0,16},{4,20},{8,24},{12,28},{16,0},{20,4},{24,8},{28,12},{1,17},{... | collective-permute-start | bytes 393224 | tf_op jit(solution)/shard_map/ppermute | solution.py:19
  238.8 9.1 %collective-permute-done.46 = bf16[128,512]{1,0:T(8,128)(2,1)S(1)} collective-permute-done((bf16[128,512]{1,0:T(8,128)(2,1)S(1)}, bf16[128,512]{1,0:T(8,128)(2,1)S(1)}, u32[]{:S(2)}, u32[]{:S(2)}) %collective-permute-start.46) | collective-permute-done | bytes 131104 | tf_op jit(solution)/shard_map/ppermute | solution.py:19
  (208 shorter events, 67.1 us)
Async XLA Ops:
  18.0 14.9 %collective-permute-start.3 = (bf16[4,32,2048]{2,1,0:T(8,128)(2,1)S(1)}, bf16[4,32,2048]{2,1,0:T(8,128)(2,1)S(1)}, u32[]{:S(2)}, u32[]{:S(2)}) collective-permute-start(bf16[4,32,2048]{2,1,0:T(8,128)(2,1)S(1)} %pad_maximum_fusion.refs_0_), channel_id=1, source_target_pairs={{0,1},{1,0},{2,3},{3,2},{4,5},{5,4},{6,7},{7,6},{8,9},{9,8},{10,11... | collective-permute-start | bytes 1572872 | tf_op jit(solution)/shard_map/ppermute | solution.py:19
  19.5 23.9 %collective-permute-start.4 = (bf16[4,32,2048]{2,1,0:T(8,128)(2,1)S(1)}, bf16[4,32,2048]{2,1,0:T(8,128)(2,1)S(1)}, u32[]{:S(2)}, u32[]{:S(2)}) collective-permute-start(bf16[4,32,2048]{2,1,0:T(8,128)(2,1)S(1)} %pad_maximum_fusion.refs_0_), channel_id=1, source_target_pairs={{0,2},{1,3},{2,0},{3,1},{4,6},{5,7},{6,4},{7,5},{8,10},{9,11},{10,... | collective-permute-start | bytes 1572872 | tf_op jit(solution)/shard_map/ppermute | solution.py:19
  21.1 23.2 %collective-permute-start.5 = (bf16[4,32,2048]{2,1,0:T(8,128)(2,1)S(1)}, bf16[4,32,2048]{2,1,0:T(8,128)(2,1)S(1)}, u32[]{:S(2)}, u32[]{:S(2)}) collective-permute-start(bf16[4,32,2048]{2,1,0:T(8,128)(2,1)S(1)} %pad_maximum_fusion.refs_0_), channel_id=1, source_target_pairs={{0,3},{1,2},{2,1},{3,0},{4,7},{5,6},{6,5},{7,4},{8,11},{9,10},{10,... | collective-permute-start | bytes 1572872 | tf_op jit(solution)/shard_map/ppermute | solution.py:19
  49.5 105.8 %collective-permute-start.6 = (bf16[512,2048]{1,0:T(8,128)(2,1)S(1)}, bf16[512,2048]{1,0:T(8,128)(2,1)}, u32[]{:S(2)}, u32[]{:S(2)}) collective-permute-start(bf16[512,2048]{1,0:T(8,128)(2,1)S(1)} %bitcast.30), channel_id=1, source_target_pairs={{0,4},{4,0},{8,12},{12,8},{16,20},{20,16},{24,28},{28,24},{1,5},{5... | collective-permute-start | bytes 6291464 | tf_op jit(solution)/shard_map/ppermute | solution.py:19
  49.5 12.5 %collective-permute-start.42 = (f32[8,128]{1,0:T(8,128)S(1)}, f32[8,128]{1,0:T(8,128)S(1)}, u32[]{:S(2)}, u32[]{:S(2)}) collective-permute-start(f32[8,128]{1,0:T(8,128)S(1)} %bitcast.42), channel_id=1, source_target_pairs={{0,24},{4,28},{8,16},{12,20},{16,8},{20,12},{24,0},{28,4},{1,25},{... | collective-permute-start | bytes 12296 | tf_op jit(solution)/shard_map/ppermute | solution.py:19
  65.5 13.0 %collective-permute-start.10 = (bf16[256,256]{1,0:T(8,128)(2,1)}, bf16[256,256]{1,0:T(8,128)(2,1)S(1)}, u32[]{:S(2)}, u32[]{:S(2)}) collective-permute-start(bf16[256,256]{1,0:T(8,128)(2,1)} %get-tuple-element.46), channel_id=1, source_target_pairs={{0,16},{4,20},{8,24},{12,28},{16,0},{20,4},{24,8},{28,12},{1,17},{... | collective-permute-start | bytes 393224 | tf_op jit(solution)/shard_map/ppermute | solution.py:19
  68.0 12.1 %collective-permute-start.11 = (bf16[256,256]{1,0:T(8,128)(2,1)}, bf16[256,256]{1,0:T(8,128)(2,1)S(1)}, u32[]{:S(2)}, u32[]{:S(2)}) collective-permute-start(bf16[256,256]{1,0:T(8,128)(2,1)} %get-tuple-element.47), channel_id=1, source_target_pairs={{0,20},{4,16},{8,28},{12,24},{16,4},{20,0},{24,12},{28,8},{1,21},{... | collective-permute-start | bytes 393224 | tf_op jit(solution)/shard_map/ppermute | solution.py:19
  80.8 15.5 %collective-permute-start.17 = (bf16[256,256]{1,0:T(8,128)(2,1)}, bf16[256,256]{1,0:T(8,128)(2,1)S(1)}, u32[]{:S(2)}, u32[]{:S(2)}) collective-permute-start(bf16[256,256]{1,0:T(8,128)(2,1)} %get-tuple-element.54), channel_id=1, source_target_pairs={{0,16},{4,20},{8,24},{12,28},{16,0},{20,4},{24,8},{28,12},{1,17},{... | collective-permute-start | bytes 393224 | tf_op jit(solution)/shard_map/ppermute | solution.py:19
  81.6 17.1 %collective-permute-start.18 = (bf16[256,256]{1,0:T(8,128)(2,1)}, bf16[256,256]{1,0:T(8,128)(2,1)S(1)}, u32[]{:S(2)}, u32[]{:S(2)}) collective-permute-start(bf16[256,256]{1,0:T(8,128)(2,1)} %get-tuple-element.55), channel_id=1, source_target_pairs={{0,20},{4,16},{8,28},{12,24},{16,4},{20,0},{24,12},{28,8},{1,21},{... | collective-permute-start | bytes 393224 | tf_op jit(solution)/shard_map/ppermute | solution.py:19
  84.7 14.6 %collective-permute-start.19 = (bf16[256,256]{1,0:T(8,128)(2,1)}, bf16[256,256]{1,0:T(8,128)(2,1)S(1)}, u32[]{:S(2)}, u32[]{:S(2)}) collective-permute-start(bf16[256,256]{1,0:T(8,128)(2,1)} %get-tuple-element.56), channel_id=1, source_target_pairs={{0,24},{4,28},{8,16},{12,20},{16,8},{20,12},{24,0},{28,4},{1,25},{... | collective-permute-start | bytes 393224 | tf_op jit(solution)/shard_map/ppermute | solution.py:19
  87.7 26.1 %collective-permute-start.21 = (bf16[256,512]{1,0:T(8,128)(2,1)}, bf16[256,512]{1,0:T(8,128)(2,1)S(1)}, u32[]{:S(2)}, u32[]{:S(2)}) collective-permute-start(bf16[256,512]{1,0:T(8,128)(2,1)} %get-tuple-element.59), channel_id=1, source_target_pairs={{0,4},{4,0},{8,12},{12,8},{16,20},{20,16},{24,28},{28,24},{1,5},{5... | collective-permute-start | bytes 786440 | tf_op jit(solution)/shard_map/ppermute | solution.py:19
  97.0 19.5 %collective-permute-start.22 = (bf16[256,512]{1,0:T(8,128)(2,1)}, bf16[256,512]{1,0:T(8,128)(2,1)S(1)}, u32[]{:S(2)}, u32[]{:S(2)}) collective-permute-start(bf16[256,512]{1,0:T(8,128)(2,1)} %get-tuple-element.60), channel_id=1, source_target_pairs={{0,8},{4,12},{8,0},{12,4},{16,24},{20,28},{24,16},{28,20},{1,9},{5... | collective-permute-start | bytes 786440 | tf_op jit(solution)/shard_map/ppermute | solution.py:19
  99.4 19.7 %collective-permute-start.23 = (bf16[256,512]{1,0:T(8,128)(2,1)}, bf16[256,512]{1,0:T(8,128)(2,1)S(1)}, u32[]{:S(2)}, u32[]{:S(2)}) collective-permute-start(bf16[256,512]{1,0:T(8,128)(2,1)} %get-tuple-element.61), channel_id=1, source_target_pairs={{0,12},{4,8},{8,4},{12,0},{16,28},{20,24},{24,20},{28,16},{1,13},{... | collective-permute-start | bytes 786440 | tf_op jit(solution)/shard_map/ppermute | solution.py:19
  100.0 13.1 %collective-permute-start.20 = (bf16[256,256]{1,0:T(8,128)(2,1)}, bf16[256,256]{1,0:T(8,128)(2,1)S(1)}, u32[]{:S(2)}, u32[]{:S(2)}) collective-permute-start(bf16[256,256]{1,0:T(8,128)(2,1)} %get-tuple-element.57), channel_id=1, source_target_pairs={{0,28},{4,24},{8,20},{12,16},{16,12},{20,8},{24,4},{28,0},{1,29},{... | collective-permute-start | bytes 393224 | tf_op jit(solution)/shard_map/ppermute | solution.py:19
  113.8 31.4 %collective-permute-start.24 = (bf16[256,512]{1,0:T(8,128)(2,1)}, bf16[256,512]{1,0:T(8,128)(2,1)}, u32[]{:S(2)}, u32[]{:S(2)}) collective-permute-start(bf16[256,512]{1,0:T(8,128)(2,1)} %get-tuple-element.62), channel_id=1, source_target_pairs={{0,16},{4,20},{8,24},{12,28},{16,0},{20,4},{24,8},{28,12},{1,17},{... | collective-permute-start | bytes 786440 | tf_op jit(solution)/shard_map/ppermute | solution.py:19
  113.8 37.0 %collective-permute-start.25 = (bf16[256,512]{1,0:T(8,128)(2,1)}, bf16[256,512]{1,0:T(8,128)(2,1)}, u32[]{:S(2)}, u32[]{:S(2)}) collective-permute-start(bf16[256,512]{1,0:T(8,128)(2,1)} %get-tuple-element.63), channel_id=1, source_target_pairs={{0,20},{4,16},{8,28},{12,24},{16,4},{20,0},{24,12},{28,8},{1,21},{... | collective-permute-start | bytes 786440 | tf_op jit(solution)/shard_map/ppermute | solution.py:19
  117.2 35.1 %collective-permute-start.26 = (bf16[256,512]{1,0:T(8,128)(2,1)}, bf16[256,512]{1,0:T(8,128)(2,1)S(1)}, u32[]{:S(2)}, u32[]{:S(2)}) collective-permute-start(bf16[256,512]{1,0:T(8,128)(2,1)} %get-tuple-element.64), channel_id=1, source_target_pairs={{0,24},{4,28},{8,16},{12,20},{16,8},{20,12},{24,0},{28,4},{1,25},{... | collective-permute-start | bytes 786440 | tf_op jit(solution)/shard_map/ppermute | solution.py:19
  119.7 34.7 %collective-permute-start.27 = (bf16[256,512]{1,0:T(8,128)(2,1)}, bf16[256,512]{1,0:T(8,128)(2,1)S(1)}, u32[]{:S(2)}, u32[]{:S(2)}) collective-permute-start(bf16[256,512]{1,0:T(8,128)(2,1)} %get-tuple-element.65), channel_id=1, source_target_pairs={{0,28},{4,24},{8,20},{12,16},{16,12},{20,8},{24,4},{28,0},{1,29},{... | collective-permute-start | bytes 786440 | tf_op jit(solution)/shard_map/ppermute | solution.py:19
  145.3 22.1 %collective-permute-start.31 = (bf16[512,512]{1,0:T(8,128)(2,1)S(1)}, bf16[512,512]{1,0:T(8,128)(2,1)S(1)}, u32[]{:S(2)}, u32[]{:S(2)}) collective-permute-start(bf16[512,512]{1,0:T(8,128)(2,1)S(1)} %get-tuple-element.83), channel_id=1, source_target_pairs={{0,1},{1,0},{2,3},{3,2},{4,5},{5,4},{6,7},{7,6},{8,9},{9,8},{10,11... | collective-permute-start | bytes 1572872 | tf_op jit(solution)/shard_map/ppermute | solution.py:19
  150.8 26.0 %collective-permute-start.32 = (bf16[512,512]{1,0:T(8,128)(2,1)S(1)}, bf16[512,512]{1,0:T(8,128)(2,1)S(1)}, u32[]{:S(2)}, u32[]{:S(2)}) collective-permute-start(bf16[512,512]{1,0:T(8,128)(2,1)S(1)} %get-tuple-element.82), channel_id=1, source_target_pairs={{0,2},{1,3},{2,0},{3,1},{4,6},{5,7},{6,4},{7,5},{8,10},{9,11},{10,... | collective-permute-start | bytes 1572872 | tf_op jit(solution)/shard_map/ppermute | solution.py:19
  152.3 11.7 %collective-permute-start.12 = (bf16[256,256]{1,0:T(8,128)(2,1)S(1)}, bf16[256,256]{1,0:T(8,128)(2,1)S(1)}, u32[]{:S(2)}, u32[]{:S(2)}) collective-permute-start(bf16[256,256]{1,0:T(8,128)(2,1)S(1)} %copy-done.61), channel_id=1, source_target_pairs={{0,24},{4,28},{8,16},{12,20},{16,8},{20,12},{24,0},{28,4},{1,25},{... | collective-permute-start | bytes 393224 | tf_op jit(solution)/shard_map/ppermute | solution.py:19
  154.5 11.8 %collective-permute-start.13 = (bf16[256,256]{1,0:T(8,128)(2,1)S(1)}, bf16[256,256]{1,0:T(8,128)(2,1)S(1)}, u32[]{:S(2)}, u32[]{:S(2)}) collective-permute-start(bf16[256,256]{1,0:T(8,128)(2,1)S(1)} %copy-done.60), channel_id=1, source_target_pairs={{0,28},{4,24},{8,20},{12,16},{16,12},{20,8},{24,4},{28,0},{1,29},{... | collective-permute-start | bytes 393224 | tf_op jit(solution)/shard_map/ppermute | solution.py:19
  155.3 23.8 %collective-permute-start.33 = (bf16[512,512]{1,0:T(8,128)(2,1)S(1)}, bf16[512,512]{1,0:T(8,128)(2,1)S(1)}, u32[]{:S(2)}, u32[]{:S(2)}) collective-permute-start(bf16[512,512]{1,0:T(8,128)(2,1)S(1)} %get-tuple-element.81), channel_id=1, source_target_pairs={{0,3},{1,2},{2,1},{3,0},{4,7},{5,6},{6,5},{7,4},{8,11},{9,10},{10,... | collective-permute-start | bytes 1572872 | tf_op jit(solution)/shard_map/ppermute | solution.py:19
  164.7 15.7 %collective-permute-start.37 = (bf16[1024,128]{1,0:T(8,128)(2,1)S(1)}, bf16[1024,128]{1,0:T(8,128)(2,1)S(1)}, u32[]{:S(2)}, u32[]{:S(2)}) collective-permute-start(bf16[1024,128]{1,0:T(8,128)(2,1)S(1)} %get-tuple-element.74.refs_4_), channel_id=1, source_target_pairs={{0,1},{1,0},{2,3},{3,2},{4,5},{5,4},{6,7},{7,6},{8,9},{9,8},{10,11... | collective-permute-start | bytes 786440 | tf_op jit(solution)/shard_map/ppermute | solution.py:19
  166.9 44.9 %collective-permute-start.34 = (bf16[1024,256]{1,0:T(8,128)(2,1)}, bf16[1024,256]{1,0:T(8,128)(2,1)}, u32[]{:S(2)}, u32[]{:S(2)}) collective-permute-start(bf16[1024,256]{1,0:T(8,128)(2,1)} %get-tuple-element.73.refs_0_), channel_id=1, source_target_pairs={{0,1},{1,0},{2,3},{3,2},{4,5},{5,4},{6,7},{7,6},{8,9},{9,8},{10,11... | collective-permute-start | bytes 1572872 | tf_op jit(solution)/shard_map/ppermute | solution.py:19
  168.2 45.3 %collective-permute-start.35 = (bf16[1024,256]{1,0:T(8,128)(2,1)}, bf16[1024,256]{1,0:T(8,128)(2,1)}, u32[]{:S(2)}, u32[]{:S(2)}) collective-permute-start(bf16[1024,256]{1,0:T(8,128)(2,1)} %get-tuple-element.73.refs_0_), channel_id=1, source_target_pairs={{0,2},{1,3},{2,0},{3,1},{4,6},{5,7},{6,4},{7,5},{8,10},{9,11},{10,... | collective-permute-start | bytes 1572872 | tf_op jit(solution)/shard_map/ppermute | solution.py:19
  177.6 35.9 %collective-permute-start.36 = (bf16[1024,256]{1,0:T(8,128)(2,1)}, bf16[1024,256]{1,0:T(8,128)(2,1)}, u32[]{:S(2)}, u32[]{:S(2)}) collective-permute-start(bf16[1024,256]{1,0:T(8,128)(2,1)} %get-tuple-element.73.refs_0_), channel_id=1, source_target_pairs={{0,3},{1,2},{2,1},{3,0},{4,7},{5,6},{6,5},{7,4},{8,11},{9,10},{10,... | collective-permute-start | bytes 1572872 | tf_op jit(solution)/shard_map/ppermute | solution.py:19
  179.9 29.8 %collective-permute-start.38 = (bf16[1024,128]{1,0:T(8,128)(2,1)S(1)}, bf16[1024,128]{1,0:T(8,128)(2,1)}, u32[]{:S(2)}, u32[]{:S(2)}) collective-permute-start(bf16[1024,128]{1,0:T(8,128)(2,1)S(1)} %get-tuple-element.74.refs_4_), channel_id=1, source_target_pairs={{0,2},{1,3},{2,0},{3,1},{4,6},{5,7},{6,4},{7,5},{8,10},{9,11},{10,... | collective-permute-start | bytes 786440 | tf_op jit(solution)/shard_map/ppermute | solution.py:19
  181.1 29.1 %collective-permute-start.39 = (bf16[1024,128]{1,0:T(8,128)(2,1)S(1)}, bf16[1024,128]{1,0:T(8,128)(2,1)}, u32[]{:S(2)}, u32[]{:S(2)}) collective-permute-start(bf16[1024,128]{1,0:T(8,128)(2,1)S(1)} %get-tuple-element.74.refs_4_), channel_id=1, source_target_pairs={{0,3},{1,2},{2,1},{3,0},{4,7},{5,6},{6,5},{7,4},{8,11},{9,10},{10,... | collective-permute-start | bytes 786440 | tf_op jit(solution)/shard_map/ppermute | solution.py:19
  210.2 12.3 %collective-permute-start.29 = (bf16[1024,128]{1,0:T(8,128)(2,1)}, bf16[1024,128]{1,0:T(8,128)(2,1)}, u32[]{:S(2)}, u32[]{:S(2)}) collective-permute-start(bf16[1024,128]{1,0:T(8,128)(2,1)} %get-tuple-element.72.refs_0_), channel_id=1, source_target_pairs={{0,2},{1,3},{2,0},{3,1},{4,6},{5,7},{6,4},{7,5},{8,10},{9,11},{10,... | collective-permute-start | bytes 786440 | tf_op jit(solution)/shard_map/ppermute | solution.py:19
  211.8 12.3 %collective-permute-start.30 = (bf16[1024,128]{1,0:T(8,128)(2,1)}, bf16[1024,128]{1,0:T(8,128)(2,1)}, u32[]{:S(2)}, u32[]{:S(2)}) collective-permute-start(bf16[1024,128]{1,0:T(8,128)(2,1)} %get-tuple-element.72.refs_0_), channel_id=1, source_target_pairs={{0,3},{1,2},{2,1},{3,0},{4,7},{5,6},{6,5},{7,4},{8,11},{9,10},{10,... | collective-permute-start | bytes 786440 | tf_op jit(solution)/shard_map/ppermute | solution.py:19
  230.4 17.6 %collective-permute-start.46 = (bf16[128,512]{1,0:T(8,128)(2,1)S(1)}, bf16[128,512]{1,0:T(8,128)(2,1)S(1)}, u32[]{:S(2)}, u32[]{:S(2)}) collective-permute-start(bf16[128,512]{1,0:T(8,128)(2,1)S(1)} %get-tuple-element.79), channel_id=1, source_target_pairs={{0,16},{4,20},{8,24},{12,28},{16,0},{20,4},{24,8},{28,12},{1,17},{... | collective-permute-start | bytes 393224 | tf_op jit(solution)/shard_map/ppermute | solution.py:19
  (78 other events, 532.1 us)

commit v2 on v1

--- a/solution.py
+++ b/solution.py
@@ -10,7 +10,7 @@
 lanes = 128
 
 
-HBM = pl.BlockSpec(memory_space=pl.ANY)
+HBM = pl.BlockSpec(memory_space=pltpu.HBM)
 VMEM = pl.BlockSpec(memory_space=pltpu.VMEM)
 SMEM = pl.BlockSpec(memory_space=pltpu.SMEM)
 
@@ -20,10 +20,7 @@
 
 
 def chunk_widths(hidden):
-    count = hidden // lanes
-    if count >= 3:
-        return [hidden - 2 * lanes, lanes, lanes]
-    return [lanes] * count
+    return [lanes] * (hidden // lanes)
 
 
 def grant(used):
@@ -164,62 +161,108 @@
     )(place, *shares)
 
 
-def project(actives, downs, offsets, running, scale):
-    count, chunks = len(downs), len(actives)
-    total = actives[0][0].shape[0]
+def load_sides(down_refs, sides, sems, offsets):
+    loads = []
+    for c, offset in enumerate(offsets):
+        width = sides[c].shape[1] // len(down_refs)
+        for q, ref in enumerate(down_refs):
+            copy = pltpu.make_async_copy(
+                ref.at[:, pl.ds(offset, width)], sides[c].at[:, pl.ds(q * width, width)], sems.at[c, q]
+            )
+            copy.start()
+            loads.append(copy)
+    return loads
+
+
+def contract(active_refs, span, side):
+    left = jnp.concatenate([a[span, :] for a in active_refs], axis=1)
+    return lax.dot_general(left, side, (((1,), (1,)), ((), ())), preferred_element_type=jnp.float32)
+
+
+def project_early(actives, downs, scale, offsets, widths):
+    count, chunks, early = len(downs), len(widths), len(actives)
     features = downs[0].shape[0]
-    widths = [group[0].shape[1] for group in actives]
+    total = scale.shape[0]
     block = min(256, total)
-    blocks = total // block
-    extra = ([running] if running is not None else []) + ([scale] if scale is not None else [])
 
     def kernel(*refs):
-        active_refs = [refs[c * count : (c + 1) * count] for c in range(chunks)]
-        down_refs = refs[chunks * count : (chunks + 1) * count]
-        others = refs[(chunks + 1) * count :]
-        sides = [
-            jnp.concatenate([d[:, o : o + w] for d in down_refs], axis=1) for o, w in zip(offsets, widths)
-        ]
-        for n in range(blocks):
+        groups = [refs[c * count : (c + 1) * count] for c in range(early)]
+        down_refs = refs[early * count : (early + 1) * count]
+        scale_ref = refs[(early + 1) * count]
+        outs = refs[(early + 1) * count + 1 :][: len(shapes)]
+        *sides, sems = refs[(early + 1) * count + 1 + len(shapes) :]
+        loads = load_sides(down_refs, [*sides, *outs[: chunks - early]], sems, offsets)
+        outs[chunks - early][...] = scale_ref[...]
+        for copy in loads:
+            copy.wait()
+        if not early:
+            return
+        for n in range(total // block):
             span = slice(n * block, (n + 1) * block)
-            acc = others[0][span, :] if running is not None else None
-            for c in range(chunks):
-                left = jnp.concatenate([a[span, :] for a in active_refs[c]], axis=1)
-                part = lax.dot_general(
-                    left, sides[c], (((1,), (1,)), ((), ())), preferred_element_type=jnp.float32
-                )
+            acc = None
+            for c in range(early):
+                part = contract(groups[c], span, sides[c][...])
                 acc = part if acc is None else acc + part
-            if scale is None:
-                others[-1][span, :] = acc
-            else:
-                acc = acc * others[len(extra) - 1][span, :]
-                if n < blocks // 2:
-                    others[-2][span, :] = acc
-                else:
-                    others[-1][slice(n * block - total // 2, (n + 1) * block - total // 2), :] = acc.astype(
-                        jnp.bfloat16
-                    )
-
-    if scale is None:
-        shapes = jax.ShapeDtypeStruct((total, features), jnp.float32)
-        specs = VMEM
-    else:
-        shapes = [
-            jax.ShapeDtypeStruct((total // 2, features), jnp.float32),
-            jax.ShapeDtypeStruct((total // 2, features), jnp.bfloat16),
-        ]
-        specs = [VMEM, VMEM]
+            outs[-1][span, :] = acc
+
+    shapes = [jax.ShapeDtypeStruct((features, count * w), jnp.bfloat16) for w in widths[early:]]
+    shapes.append(jax.ShapeDtypeStruct(scale.shape, jnp.float32))
+    if early:
+        shapes.append(jax.ShapeDtypeStruct((total, features), jnp.float32))
     return pl.pallas_call(
         kernel,
         out_shape=shapes,
-        in_specs=[VMEM] * ((chunks + 1) * count + len(extra)),
-        out_specs=specs,
+        in_specs=[VMEM] * (early * count) + [HBM] * count + [VMEM],
+        out_specs=[VMEM] * len(shapes),
+        scratch_shapes=[
+            *[pltpu.VMEM((features, count * w), jnp.bfloat16) for w in widths[:early]],
+            pltpu.SemaphoreType.DMA((chunks, count)),
+        ],
         compiler_params=grant(
-            2 * count * total * sum(widths) + 4 * features * sum(d.shape[1] for d in downs) + 12 * total * features
+            2 * count * total * sum(widths) + 2 * features * count * sum(widths) + 8 * total * features
         ),
         cost_estimate=cost(2 * total * features * count * sum(widths), 4 * total * features),
         name="project",
-    )(*[a for group in actives for a in group], *downs, *extra)
+    )(*[a for group in actives for a in group], *downs, scale)
+
+
+def project_late(actives, sides, running, scale):
+    count, late = len(actives[0]), len(actives)
+    total = actives[0][0].shape[0]
+    features = sides[0].shape[0]
+    block = min(256, total // 2)
+    blocks = total // block
+    depth = sum(side.shape[1] for side in sides)
+
+    def kernel(*refs):
+        groups = [refs[c * count : (c + 1) * count] for c in range(late)]
+        side_refs = refs[late * count : late * count + late]
+        scale_ref, *rest = refs[late * count + late :]
+        kept_ref, sent_ref = rest[-2:]
+        for n in reversed(range(blocks)):
+            span = slice(n * block, (n + 1) * block)
+            acc = rest[0][span, :] if running else None
+            for c in range(late):
+                part = contract(groups[c], span, side_refs[c][...])
+                acc = part if acc is None else acc + part
+            acc = acc * scale_ref[span, :]
+            if n < blocks // 2:
+                kept_ref[span, :] = acc
+            else:
+                sent_ref[slice(n * block - total // 2, (n + 1) * block - total // 2), :] = acc.astype(jnp.bfloat16)
+
+    return pl.pallas_call(
+        kernel,
+        out_shape=[
+            jax.ShapeDtypeStruct((total // 2, features), jnp.float32),
+            jax.ShapeDtypeStruct((total // 2, features), jnp.bfloat16),
+        ],
+        in_specs=[VMEM] * (late * (count + 1) + 1 + len(running)),
+        out_specs=[VMEM] * 2,
+        compiler_params=grant(2 * total * depth + 2 * features * depth + 10 * total * features),
+        cost_estimate=cost(2 * total * features * depth, 4 * total * features),
+        name="project",
+    )(*[a for group in actives for a in group], *sides, scale, *running)
 
 
 def combine(kept, arrived, groups):
@@ -259,7 +302,8 @@
 
         share = lax.dynamic_slice_in_dim(tokens, j * sub, sub, 0)
         shares = jnp.stack([share] + [swap(share, "fs", n_fs, 2 * k) for k in range(1, n_z)])
-        near = assemble(place, [shares] + [swap(shares, "tp", n_tp, q) for q in range(1, n_tp)])
+        shares = [shares] + [swap(shares, "tp", n_tp, q) for q in range(1, n_tp)]
+        near = assemble(place, shares)
         near = near.reshape(n_z * tok_count, width)
         far = swap(near, "fs", n_fs, 1)
 
@@ -281,14 +325,14 @@
 
         built = []
         actives = []
-        running = None
         for c in range(len(widths)):
             active, *built = activate(place, [near, far], arrived[c], built, offsets[c], hidden)
             actives.append([active] + [swap(active, "tp", n_tp, q) for q in range(1, n_tp)])
 
-        if len(widths) > 1:
-            running = project(actives[:-1], downs, offsets[:-1], None, None)
-        kept, sent = project(actives[-1:], downs, offsets[-1:], running, scale)
+        early = max(0, len(widths) - 2)
+        rest = project_early(actives[:early], downs, scale, offsets, widths)
+        sides, scale, running = rest[: len(widths) - early], rest[len(widths) - early], rest[len(widths) - early + 1 :]
+        kept, sent = project_late(actives[early:], sides, running, scale)
         own, *others = combine(kept, swap(sent, "fs", n_fs, 1), n_z)
         total = own
         for k, other in enumerate(others, 1):

time: 249 us -> 251 us (level)
  waiting for transfers between devices: 126 us -> 104 us
  starting transfers between devices: 59.6 us -> 74.2 us
  Pallas kernels: 25.4 us -> 29.5 us
  local copies, waits for them, and re-layouts: 35.5 us -> 39.3 us
    ppermute x48 -> x58, waiting for transfers between devices: 126 us -> 104 us  [swap(): return lax.ppermute(value, axis, [(i, i ^ step) for i in range(size)])]
    ppermute x48 -> x58, starting transfers between devices: 59.6 us -> 74.2 us  [swap(): return lax.ppermute(value, axis, [(i, i ^ step) for i in range(size)])]
    pallas_call x3 -> x4, Pallas kernels: 12.7 us -> 16.6 us  [activate(): pl.pallas_call(kernel, out_shape=[jax.ShapeDtypeStruct((total, width), jn...]
    unnamed x124 -> x144, local copies, waits for them, and re-layouts: 31.9 us -> 35.7 us
  transfers between devices with their start and end apart: 48 -> 58, of which waited for: 19 -> 24; matrix products, arithmetic and copies ran while one was open for 2% -> 2% of each run, Pallas kernels for 9% -> 11%
where the time goes in v2:
time: 251 us; the launch traced here: 250 us
  waiting for transfers between devices  104 us (41%)
  starting transfers between devices  74.2 us (30%)
  local copies, waits for them, and re-layouts  39.3 us (16%)
  Pallas kernels  29.5 us (12%)
    ppermute x58, waiting for transfers between devices, swap(): return lax.ppermute(value, axis, [(i, i ^ step) for i in range(size)])  104 us
    ppermute x58, starting transfers between devices, swap(): return lax.ppermute(value, axis, [(i, i ^ step) for i in range(size)])  74.2 us
    unnamed x144, local copies, waits for them, and re-layouts  35.7 us
    pallas_call x4, Pallas kernels, activate(): pl.pallas_call(kernel, out_shape=[jax.ShapeDtypeStruct((total, width), jn...  16.6 us
    pallas_call x1, Pallas kernels, convert(): pl.pallas_call(kernel, out_shape=[jax.ShapeDtypeStruct((rows, 2 * width),...  6.48 us
  transfers between devices with their start and end apart: 58, of which 24 were waited for; matrix products, arithmetic and copies ran while one was open for 2% of the time, Pallas kernels for 11%

profile of v2, /device:TPU:0, one launch (start us, length us, event | category | flops | bytes accessed | tf_op | source)
XLA Modules:
  0.0 249.7 jit_solution(10530354811636336500)
XLA Ops:
  1.7 5.1 %collective-permute-start.2 = (bf16[32,2048]{1,0:T(8,128)(2,1)S(1)}, bf16[32,2048]{1,0:T(8,128)(2,1)S(1)}, u32[]{:S(2)}, u32[]{:S(2)}) collective-permute-start(bf16[32,2048]{1,0:T(8,128)(2,1)S(1)} %constant_dynamic-slice_fusion), channel_id=1, source_target_pairs={{0,24},{4,28},{8,16},{12,20},{16,8},{20,12},{24,0},{28,4},{1,25},{... | collective-permute-start | bytes 393224 | tf_op jit(solution)/shard_map/ppermute | solution.py:19
  7.5 3.8 %collective-permute-done.2 = bf16[32,2048]{1,0:T(8,128)(2,1)S(1)} collective-permute-done((bf16[32,2048]{1,0:T(8,128)(2,1)S(1)}, bf16[32,2048]{1,0:T(8,128)(2,1)S(1)}, u32[]{:S(2)}, u32[]{:S(2)}) %collective-permute-start.2) | collective-permute-done | bytes 131104 | tf_op jit(solution)/shard_map/ppermute | solution.py:19
  11.3 6.6 %collective-permute-done.1 = bf16[32,2048]{1,0:T(8,128)(2,1)S(1)} collective-permute-done((bf16[32,2048]{1,0:T(8,128)(2,1)S(1)}, bf16[32,2048]{1,0:T(8,128)(2,1)S(1)}, u32[]{:S(2)}, u32[]{:S(2)}) %collective-permute-start.1) | collective-permute-done | bytes 131104 | tf_op jit(solution)/shard_map/ppermute | solution.py:19
  21.6 11.2 %collective-permute-done.3.refs_1_ = bf16[4,32,2048]{2,1,0:T(8,128)(2,1)S(1)} collective-permute-done((bf16[4,32,2048]{2,1,0:T(8,128)(2,1)S(1)}, bf16[4,32,2048]{2,1,0:T(8,128)(2,1)S(1)}, u32[]{:S(2)}, u32[]{:S(2)}) %collective-permute-start.3) | collective-permute-done | bytes 524320 | tf_op jit(solution)/shard_map/ppermute | solution.py:19
  33.6 9.9 %collective-permute-done.4.refs_2_ = bf16[4,32,2048]{2,1,0:T(8,128)(2,1)S(1)} collective-permute-done((bf16[4,32,2048]{2,1,0:T(8,128)(2,1)S(1)}, bf16[4,32,2048]{2,1,0:T(8,128)(2,1)S(1)}, u32[]{:S(2)}, u32[]{:S(2)}) %collective-permute-start.4) | collective-permute-done | bytes 524320 | tf_op jit(solution)/shard_map/ppermute | solution.py:19
  49.5 2.4 collective-permute-start.52
  51.9 2.1 collective-permute-start.50
  55.5 6.5 %convert.1 = (bf16[256,256]{1,0:T(8,128)(2,1)}, bf16[256,256]{1,0:T(8,128)(2,1)}, bf16[256,256]{1,0:T(8,128)(2,1)}, bf16[256,256]{1,0:T(8,128)(2,1)}, bf16[256,2...) custom-call(s32[2]{0:T(128)} %copy-done.55, ...), custom_call_target="tpu_custom_call" | custom-call | flops 4194304 | bytes 12582912 | tf_op jit(solution)/shard_map/convert/pallas_call | solution.py:71
  69.9 2.8 %collective-permute-done.9.refs_3_ = bf16[256,256]{1,0:T(8,128)(2,1)S(1)} collective-permute-done((bf16[256,256]{1,0:T(8,128)(2,1)}, bf16[256,256]{1,0:T(8,128)(2,1)S(1)}, u32[]{:S(2)}, u32[]{:S(2)}) %collective-permute-start.9) | collective-permute-done | bytes 131104 | tf_op jit(solution)/shard_map/ppermute | solution.py:19
  73.6 5.0 %collective-permute-done.10.refs_4_ = bf16[256,256]{1,0:T(8,128)(2,1)S(1)} collective-permute-done((bf16[256,256]{1,0:T(8,128)(2,1)}, bf16[256,256]{1,0:T(8,128)(2,1)S(1)}, u32[]{:S(2)}, u32[]{:S(2)}) %collective-permute-start.10) | collective-permute-done | bytes 131104 | tf_op jit(solution)/shard_map/ppermute | solution.py:19
  81.7 2.5 collective-permute-start.18
  84.8 2.3 collective-permute-start.19
  89.0 10.2 %collective-permute-done.17.refs_4_ = bf16[256,256]{1,0:T(8,128)(2,1)S(1)} collective-permute-done((bf16[256,256]{1,0:T(8,128)(2,1)}, bf16[256,256]{1,0:T(8,128)(2,1)S(1)}, u32[]{:S(2)}, u32[]{:S(2)}) %collective-permute-start.17) | collective-permute-done | bytes 131104 | tf_op jit(solution)/shard_map/ppermute | solution.py:19
  102.9 2.4 collective-permute-start.23
  106.0 3.0 %collective-permute-start.24 = (bf16[256,256]{1,0:T(8,128)(2,1)}, bf16[256,256]{1,0:T(8,128)(2,1)S(1)}, u32[]{:S(2)}, u32[]{:S(2)}) collective-permute-start(bf16[256,256]{1,0:T(8,128)(2,1)} %get-tuple-element.77), channel_id=1, source_target_pairs={{0,16},{4,20},{8,24},{12,28},{16,0},{20,4},{24,8},{28,12},{1,17},{... | collective-permute-start | bytes 393224 | tf_op jit(solution)/shard_map/ppermute | solution.py:19
  112.0 7.2 %collective-permute-done.24.refs_4_ = bf16[256,256]{1,0:T(8,128)(2,1)S(1)} collective-permute-done((bf16[256,256]{1,0:T(8,128)(2,1)}, bf16[256,256]{1,0:T(8,128)(2,1)S(1)}, u32[]{:S(2)}, u32[]{:S(2)}) %collective-permute-start.24) | collective-permute-done | bytes 131104 | tf_op jit(solution)/shard_map/ppermute | solution.py:19
  122.9 2.4 collective-permute-start.32
  128.1 2.2 collective-permute-start.27
  130.4 9.5 %collective-permute-done.31.refs_4_ = bf16[256,256]{1,0:T(8,128)(2,1)S(1)} collective-permute-done((bf16[256,256]{1,0:T(8,128)(2,1)}, bf16[256,256]{1,0:T(8,128)(2,1)S(1)}, u32[]{:S(2)}, u32[]{:S(2)}) %collective-permute-start.31) | collective-permute-done | bytes 131104 | tf_op jit(solution)/shard_map/ppermute | solution.py:19
  148.5 2.2 collective-permute-done.34.refs_7_
  152.7 4.5 %activate.4 = (bf16[1024,128]{1,0:T(8,128)(2,1)}, bf16[2048,512]{1,0:T(8,128)(2,1)}, bf16[2048,512]{1,0:T(8,128)(2,1)}) custom-call(s32[2]{0:T(128)S(1)} %copy-done.56, bf16[512,2048]{1,0:T(8,128)(2,1)S(1)} %bitcast.31, bf16[512,2048]{1,0:T(8,128)(2,1)} %collective-permute-done.6.xb_ref, bf16[256,256]{1,0:T(8,128)(2,1)S(1)} %copy-done.44, ...), custom_call_target="tpu_custom_call" | custom-call | flops 1073741824 | bytes 4194304 | tf_op jit(solution)/shard_map/activate/pallas_call | solution.py:127
  160.1 4.6 %activate.5 = (bf16[1024,128]{1,0:T(8,128)(2,1)}, bf16[2048,512]{1,0:T(8,128)(2,1)}, bf16[2048,512]{1,0:T(8,128)(2,1)}) custom-call(s32[2]{0:T(128)S(1)} %copy-done.56, bf16[512,2048]{1,0:T(8,128)(2,1)S(1)} %bitcast.32, bf16[512,2048]{1,0:T(8,128)(2,1)} %collective-permute-done.6.xb_ref, ...), custom_call_target="tpu_custom_call", output_to_operand_aliasing={{1}: (11, {}), {2}: (12, {})} | custom-call | flops 1073741824 | bytes 4194304 | tf_op jit(solution)/shard_map/activate/pallas_call | solution.py:127
  164.8 3.0 %activate.6 = (bf16[1024,128]{1,0:T(8,128)(2,1)S(1)}, bf16[2048,512]{1,0:T(8,128)(2,1)}, bf16[2048,512]{1,0:T(8,128)(2,1)}) custom-call(s32[2]{0:T(128)S(1)} %copy-done.56, bf16[512,2048]{1,0:T(8,128)(2,1)S(1)} %bitcast.33, bf16[512,2048]{1,0:T(8,128)(2,1)} %collective-permute-done.6.xb_ref, ...), custom_call_target="tpu_custom_call", output_to_operand_aliasing={{1}: (11, {}), {2}: (12, {})} | custom-call | flops 1073741824 | bytes 4194304 | tf_op jit(solution)/shard_map/activate/pallas_call | solution.py:127
  173.6 2.7 %collective-permute-done.48.refs_10_ = bf16[512,512]{1,0:T(8,128)(2,1)S(1)} collective-permute-done((bf16[512,512]{1,0:T(8,128)(2,1)S(1)}, bf16[512,512]{1,0:T(8,128)(2,1)S(1)}, u32[]{:S(2)}, u32[]{:S(2)}) %collective-permute-start.48) | collective-permute-done | bytes 524320 | tf_op jit(solution)/shard_map/ppermute | solution.py:19
  184.1 2.2 collective-permute-start.46
  192.6 4.5 %activate.7 = (bf16[1024,128]{1,0:T(8,128)(2,1)}, bf16[2048,512]{1,0:T(8,128)(2,1)}, bf16[2048,512]{1,0:T(8,128)(2,1)}) custom-call(s32[2]{0:T(128)S(1)} %copy-done.56, bf16[512,2048]{1,0:T(8,128)(2,1)S(1)} %bitcast.34, bf16[512,2048]{1,0:T(8,128)(2,1)} %collective-permute-done.6.xb_ref, ...), custom_call_target="tpu_custom_call", output_to_operand_aliasing={{1}: (11, {}), {2}: (12, {})} | custom-call | flops 1073741824 | bytes 4194304 | tf_op jit(solution)/shard_map/activate/pallas_call | solution.py:127
  207.2 3.3 %project.2 = (bf16[512,512]{1,0:T(8,128)(2,1)S(1)}, bf16[512,512]{1,0:T(8,128)(2,1)S(1)}, f32[1024,1]{1,0:T(8,128)S(1)}, f32[1024,512]{1,0:T(8,128)S(1)}) custom-call(bf16[1024,128]{1,0:T(8,128)(2,1)} %get-tuple-element.99.refs_0_, bf16[1024,128]{1,0:T(8,128)(2,1)S(1)} %copy-done.64, bf16[1024,128]{1,0:T(8,128)(2,1)} %collective-permute-done.42.refs_2_, ...), custom_call_target="tpu_custom_call" | custom-call | flops 2147483648 | bytes 2097152 | tf_op jit(solution)/shard_map/project/pallas_call | solution.py:212
  210.5 2.9 %collective-permute-done.36.refs_2_ = bf16[1024,128]{1,0:T(8,128)(2,1)S(1)} collective-permute-done((bf16[1024,128]{1,0:T(8,128)(2,1)S(1)}, bf16[1024,128]{1,0:T(8,128)(2,1)S(1)}, u32[]{:S(2)}, u32[]{:S(2)}) %collective-permute-start.36) | collective-permute-done | bytes 262176 | tf_op jit(solution)/shard_map/ppermute | solution.py:19
  213.5 10.3 %collective-permute-done.39.refs_6_ = bf16[1024,128]{1,0:T(8,128)(2,1)S(1)} collective-permute-done((bf16[1024,128]{1,0:T(8,128)(2,1)}, bf16[1024,128]{1,0:T(8,128)(2,1)S(1)}, u32[]{:S(2)}, u32[]{:S(2)}) %collective-permute-start.39) | collective-permute-done | bytes 262176 | tf_op jit(solution)/shard_map/ppermute | solution.py:19
  223.8 2.3 project.3
  230.1 9.7 %collective-permute-start.56 = (bf16[128,512]{1,0:T(8,128)(2,1)S(1)}, bf16[128,512]{1,0:T(8,128)(2,1)S(1)}, u32[]{:S(2)}, u32[]{:S(2)}) collective-permute-start(bf16[128,512]{1,0:T(8,128)(2,1)S(1)} %get-tuple-element.109), channel_id=1, source_target_pairs={{0,16},{4,20},{8,24},{12,28},{16,0},{20,4},{24,8},{28,12},{1,17},{... | collective-permute-start | bytes 393224 | tf_op jit(solution)/shard_map/ppermute | solution.py:19
  239.9 9.1 %collective-permute-done.56 = bf16[128,512]{1,0:T(8,128)(2,1)S(1)} collective-permute-done((bf16[128,512]{1,0:T(8,128)(2,1)S(1)}, bf16[128,512]{1,0:T(8,128)(2,1)S(1)}, u32[]{:S(2)}, u32[]{:S(2)}) %collective-permute-start.56) | collective-permute-done | bytes 131104 | tf_op jit(solution)/shard_map/ppermute | solution.py:19
  (249 shorter events, 90.1 us)
Async XLA Ops:
  18.0 14.9 %collective-permute-start.3 = (bf16[4,32,2048]{2,1,0:T(8,128)(2,1)S(1)}, bf16[4,32,2048]{2,1,0:T(8,128)(2,1)S(1)}, u32[]{:S(2)}, u32[]{:S(2)}) collective-permute-start(bf16[4,32,2048]{2,1,0:T(8,128)(2,1)S(1)} %pad_maximum_fusion.refs_0_), channel_id=1, source_target_pairs={{0,1},{1,0},{2,3},{3,2},{4,5},{5,4},{6,7},{7,6},{8,9},{9,8},{10,11... | collective-permute-start | bytes 1572872 | tf_op jit(solution)/shard_map/ppermute | solution.py:19
  19.5 23.9 %collective-permute-start.4 = (bf16[4,32,2048]{2,1,0:T(8,128)(2,1)S(1)}, bf16[4,32,2048]{2,1,0:T(8,128)(2,1)S(1)}, u32[]{:S(2)}, u32[]{:S(2)}) collective-permute-start(bf16[4,32,2048]{2,1,0:T(8,128)(2,1)S(1)} %pad_maximum_fusion.refs_0_), channel_id=1, source_target_pairs={{0,2},{1,3},{2,0},{3,1},{4,6},{5,7},{6,4},{7,5},{8,10},{9,11},{10,... | collective-permute-start | bytes 1572872 | tf_op jit(solution)/shard_map/ppermute | solution.py:19
  21.1 23.2 %collective-permute-start.5 = (bf16[4,32,2048]{2,1,0:T(8,128)(2,1)S(1)}, bf16[4,32,2048]{2,1,0:T(8,128)(2,1)S(1)}, u32[]{:S(2)}, u32[]{:S(2)}) collective-permute-start(bf16[4,32,2048]{2,1,0:T(8,128)(2,1)S(1)} %pad_maximum_fusion.refs_0_), channel_id=1, source_target_pairs={{0,3},{1,2},{2,1},{3,0},{4,7},{5,6},{6,5},{7,4},{8,11},{9,10},{10,... | collective-permute-start | bytes 1572872 | tf_op jit(solution)/shard_map/ppermute | solution.py:19
  49.5 102.7 %collective-permute-start.6 = (bf16[512,2048]{1,0:T(8,128)(2,1)S(1)}, bf16[512,2048]{1,0:T(8,128)(2,1)}, u32[]{:S(2)}, u32[]{:S(2)}) collective-permute-start(bf16[512,2048]{1,0:T(8,128)(2,1)S(1)} %bitcast.30), channel_id=1, source_target_pairs={{0,4},{4,0},{8,12},{12,8},{16,20},{20,16},{24,28},{28,24},{1,5},{5... | collective-permute-start | bytes 6291464 | tf_op jit(solution)/shard_map/ppermute | solution.py:19
  65.5 13.0 %collective-permute-start.10 = (bf16[256,256]{1,0:T(8,128)(2,1)}, bf16[256,256]{1,0:T(8,128)(2,1)S(1)}, u32[]{:S(2)}, u32[]{:S(2)}) collective-permute-start(bf16[256,256]{1,0:T(8,128)(2,1)} %get-tuple-element.61), channel_id=1, source_target_pairs={{0,16},{4,20},{8,24},{12,28},{16,0},{20,4},{24,8},{28,12},{1,17},{... | collective-permute-start | bytes 393224 | tf_op jit(solution)/shard_map/ppermute | solution.py:19
  80.8 18.3 %collective-permute-start.17 = (bf16[256,256]{1,0:T(8,128)(2,1)}, bf16[256,256]{1,0:T(8,128)(2,1)S(1)}, u32[]{:S(2)}, u32[]{:S(2)}) collective-permute-start(bf16[256,256]{1,0:T(8,128)(2,1)} %get-tuple-element.69), channel_id=1, source_target_pairs={{0,16},{4,20},{8,24},{12,28},{16,0},{20,4},{24,8},{28,12},{1,17},{... | collective-permute-start | bytes 393224 | tf_op jit(solution)/shard_map/ppermute | solution.py:19
  81.7 19.9 %collective-permute-start.18 = (bf16[256,256]{1,0:T(8,128)(2,1)}, bf16[256,256]{1,0:T(8,128)(2,1)S(1)}, u32[]{:S(2)}, u32[]{:S(2)}) collective-permute-start(bf16[256,256]{1,0:T(8,128)(2,1)} %get-tuple-element.70), channel_id=1, source_target_pairs={{0,20},{4,16},{8,28},{12,24},{16,4},{20,0},{24,12},{28,8},{1,21},{... | collective-permute-start | bytes 393224 | tf_op jit(solution)/shard_map/ppermute | solution.py:19
  84.8 17.4 %collective-permute-start.19 = (bf16[256,256]{1,0:T(8,128)(2,1)}, bf16[256,256]{1,0:T(8,128)(2,1)S(1)}, u32[]{:S(2)}, u32[]{:S(2)}) collective-permute-start(bf16[256,256]{1,0:T(8,128)(2,1)} %get-tuple-element.71), channel_id=1, source_target_pairs={{0,24},{4,28},{8,16},{12,20},{16,8},{20,12},{24,0},{28,4},{1,25},{... | collective-permute-start | bytes 393224 | tf_op jit(solution)/shard_map/ppermute | solution.py:19
  87.7 17.6 %collective-permute-start.20 = (bf16[256,256]{1,0:T(8,128)(2,1)}, bf16[256,256]{1,0:T(8,128)(2,1)S(1)}, u32[]{:S(2)}, u32[]{:S(2)}) collective-permute-start(bf16[256,256]{1,0:T(8,128)(2,1)} %get-tuple-element.72), channel_id=1, source_target_pairs={{0,28},{4,24},{8,20},{12,16},{16,12},{20,8},{24,4},{28,0},{1,29},{... | collective-permute-start | bytes 393224 | tf_op jit(solution)/shard_map/ppermute | solution.py:19
  106.0 13.2 %collective-permute-start.24 = (bf16[256,256]{1,0:T(8,128)(2,1)}, bf16[256,256]{1,0:T(8,128)(2,1)S(1)}, u32[]{:S(2)}, u32[]{:S(2)}) collective-permute-start(bf16[256,256]{1,0:T(8,128)(2,1)} %get-tuple-element.77), channel_id=1, source_target_pairs={{0,16},{4,20},{8,24},{12,28},{16,0},{20,4},{24,8},{28,12},{1,17},{... | collective-permute-start | bytes 393224 | tf_op jit(solution)/shard_map/ppermute | solution.py:19
  109.0 12.6 %collective-permute-start.25 = (bf16[256,256]{1,0:T(8,128)(2,1)}, bf16[256,256]{1,0:T(8,128)(2,1)S(1)}, u32[]{:S(2)}, u32[]{:S(2)}) collective-permute-start(bf16[256,256]{1,0:T(8,128)(2,1)} %get-tuple-element.78), channel_id=1, source_target_pairs={{0,20},{4,16},{8,28},{12,24},{16,4},{20,0},{24,12},{28,8},{1,21},{... | collective-permute-start | bytes 393224 | tf_op jit(solution)/shard_map/ppermute | solution.py:19
  109.1 13.2 %collective-permute-start.28 = (bf16[256,256]{1,0:T(8,128)(2,1)}, bf16[256,256]{1,0:T(8,128)(2,1)S(1)}, u32[]{:S(2)}, u32[]{:S(2)}) collective-permute-start(bf16[256,256]{1,0:T(8,128)(2,1)} %get-tuple-element.82), channel_id=1, source_target_pairs={{0,4},{4,0},{8,12},{12,8},{16,20},{20,16},{24,28},{28,24},{1,5},{5... | collective-permute-start | bytes 393224 | tf_op jit(solution)/shard_map/ppermute | solution.py:19
  110.2 15.1 %collective-permute-start.29 = (bf16[256,256]{1,0:T(8,128)(2,1)}, bf16[256,256]{1,0:T(8,128)(2,1)S(1)}, u32[]{:S(2)}, u32[]{:S(2)}) collective-permute-start(bf16[256,256]{1,0:T(8,128)(2,1)} %get-tuple-element.83), channel_id=1, source_target_pairs={{0,8},{4,12},{8,0},{12,4},{16,24},{20,28},{24,16},{28,20},{1,9},{5... | collective-permute-start | bytes 393224 | tf_op jit(solution)/shard_map/ppermute | solution.py:19
  122.2 17.7 %collective-permute-start.31 = (bf16[256,256]{1,0:T(8,128)(2,1)}, bf16[256,256]{1,0:T(8,128)(2,1)S(1)}, u32[]{:S(2)}, u32[]{:S(2)}) collective-permute-start(bf16[256,256]{1,0:T(8,128)(2,1)} %get-tuple-element.85), channel_id=1, source_target_pairs={{0,16},{4,20},{8,24},{12,28},{16,0},{20,4},{24,8},{28,12},{1,17},{... | collective-permute-start | bytes 393224 | tf_op jit(solution)/shard_map/ppermute | solution.py:19
  122.9 19.7 %collective-permute-start.32 = (bf16[256,256]{1,0:T(8,128)(2,1)}, bf16[256,256]{1,0:T(8,128)(2,1)S(1)}, u32[]{:S(2)}, u32[]{:S(2)}) collective-permute-start(bf16[256,256]{1,0:T(8,128)(2,1)} %get-tuple-element.86), channel_id=1, source_target_pairs={{0,20},{4,16},{8,28},{12,24},{16,4},{20,0},{24,12},{28,8},{1,21},{... | collective-permute-start | bytes 393224 | tf_op jit(solution)/shard_map/ppermute | solution.py:19
  125.9 31.4 %collective-permute-start.26 = (bf16[256,256]{1,0:T(8,128)(2,1)}, bf16[256,256]{1,0:T(8,128)(2,1)S(1)}, u32[]{:S(2)}, u32[]{:S(2)}) collective-permute-start(bf16[256,256]{1,0:T(8,128)(2,1)} %get-tuple-element.79), channel_id=1, source_target_pairs={{0,24},{4,28},{8,16},{12,20},{16,8},{20,12},{24,0},{28,4},{1,25},{... | collective-permute-start | bytes 393224 | tf_op jit(solution)/shard_map/ppermute | solution.py:19
  128.1 31.1 %collective-permute-start.27 = (bf16[256,256]{1,0:T(8,128)(2,1)}, bf16[256,256]{1,0:T(8,128)(2,1)S(1)}, u32[]{:S(2)}, u32[]{:S(2)}) collective-permute-start(bf16[256,256]{1,0:T(8,128)(2,1)} %get-tuple-element.80), channel_id=1, source_target_pairs={{0,28},{4,24},{8,20},{12,16},{16,12},{20,8},{24,4},{28,0},{1,29},{... | collective-permute-start | bytes 393224 | tf_op jit(solution)/shard_map/ppermute | solution.py:19
  148.0 23.1 %collective-permute-start.47 = (bf16[512,512]{1,0:T(8,128)(2,1)S(1)}, bf16[512,512]{1,0:T(8,128)(2,1)S(1)}, u32[]{:S(2)}, u32[]{:S(2)}) collective-permute-start(bf16[512,512]{1,0:T(8,128)(2,1)S(1)} %get-tuple-element.113), channel_id=1, source_target_pairs={{0,1},{1,0},{2,3},{3,2},{4,5},{5,4},{6,7},{7,6},{8,9},{9,8},{10,11... | collective-permute-start | bytes 1572872 | tf_op jit(solution)/shard_map/ppermute | solution.py:19
  150.7 25.6 %collective-permute-start.48 = (bf16[512,512]{1,0:T(8,128)(2,1)S(1)}, bf16[512,512]{1,0:T(8,128)(2,1)S(1)}, u32[]{:S(2)}, u32[]{:S(2)}) collective-permute-start(bf16[512,512]{1,0:T(8,128)(2,1)S(1)} %get-tuple-element.112), channel_id=1, source_target_pairs={{0,2},{1,3},{2,0},{3,1},{4,6},{5,7},{6,4},{7,5},{8,10},{9,11},{10,... | collective-permute-start | bytes 1572872 | tf_op jit(solution)/shard_map/ppermute | solution.py:19
  152.2 25.9 %collective-permute-start.49 = (bf16[512,512]{1,0:T(8,128)(2,1)S(1)}, bf16[512,512]{1,0:T(8,128)(2,1)S(1)}, u32[]{:S(2)}, u32[]{:S(2)}) collective-permute-start(bf16[512,512]{1,0:T(8,128)(2,1)S(1)} %get-tuple-element.111), channel_id=1, source_target_pairs={{0,3},{1,2},{2,1},{3,0},{4,7},{5,6},{6,5},{7,4},{8,11},{9,10},{10,... | collective-permute-start | bytes 1572872 | tf_op jit(solution)/shard_map/ppermute | solution.py:19
  170.7 12.6 %collective-permute-start.41 = (bf16[1024,128]{1,0:T(8,128)(2,1)}, bf16[1024,128]{1,0:T(8,128)(2,1)S(1)}, u32[]{:S(2)}, u32[]{:S(2)}) collective-permute-start(bf16[1024,128]{1,0:T(8,128)(2,1)} %get-tuple-element.99.refs_0_), channel_id=1, source_target_pairs={{0,1},{1,0},{2,3},{3,2},{4,5},{5,4},{6,7},{7,6},{8,9},{9,8},{10,11... | collective-permute-start | bytes 786440 | tf_op jit(solution)/shard_map/ppermute | solution.py:19
  172.0 25.1 %collective-permute-start.42 = (bf16[1024,128]{1,0:T(8,128)(2,1)}, bf16[1024,128]{1,0:T(8,128)(2,1)}, u32[]{:S(2)}, u32[]{:S(2)}) collective-permute-start(bf16[1024,128]{1,0:T(8,128)(2,1)} %get-tuple-element.99.refs_0_), channel_id=1, source_target_pairs={{0,2},{1,3},{2,0},{3,1},{4,6},{5,7},{6,4},{7,5},{8,10},{9,11},{10,... | collective-permute-start | bytes 786440 | tf_op jit(solution)/shard_map/ppermute | solution.py:19
  177.1 20.6 %collective-permute-start.43 = (bf16[1024,128]{1,0:T(8,128)(2,1)}, bf16[1024,128]{1,0:T(8,128)(2,1)}, u32[]{:S(2)}, u32[]{:S(2)}) collective-permute-start(bf16[1024,128]{1,0:T(8,128)(2,1)} %get-tuple-element.99.refs_0_), channel_id=1, source_target_pairs={{0,3},{1,2},{2,1},{3,0},{4,7},{5,6},{6,5},{7,4},{8,11},{9,10},{10,... | collective-permute-start | bytes 786440 | tf_op jit(solution)/shard_map/ppermute | solution.py:19
  179.0 20.4 %collective-permute-start.44 = (bf16[1024,128]{1,0:T(8,128)(2,1)}, bf16[1024,128]{1,0:T(8,128)(2,1)}, u32[]{:S(2)}, u32[]{:S(2)}) collective-permute-start(bf16[1024,128]{1,0:T(8,128)(2,1)} %get-tuple-element.100.refs_4_), channel_id=1, source_target_pairs={{0,1},{1,0},{2,3},{3,2},{4,5},{5,4},{6,7},{7,6},{8,9},{9,8},{10,11... | collective-permute-start | bytes 786440 | tf_op jit(solution)/shard_map/ppermute | solution.py:19
  181.5 19.2 %collective-permute-start.45 = (bf16[1024,128]{1,0:T(8,128)(2,1)}, bf16[1024,128]{1,0:T(8,128)(2,1)}, u32[]{:S(2)}, u32[]{:S(2)}) collective-permute-start(bf16[1024,128]{1,0:T(8,128)(2,1)} %get-tuple-element.100.refs_4_), channel_id=1, source_target_pairs={{0,2},{1,3},{2,0},{3,1},{4,6},{5,7},{6,4},{7,5},{8,10},{9,11},{10,... | collective-permute-start | bytes 786440 | tf_op jit(solution)/shard_map/ppermute | solution.py:19
  184.1 17.3 %collective-permute-start.46 = (bf16[1024,128]{1,0:T(8,128)(2,1)}, bf16[1024,128]{1,0:T(8,128)(2,1)}, u32[]{:S(2)}, u32[]{:S(2)}) collective-permute-start(bf16[1024,128]{1,0:T(8,128)(2,1)} %get-tuple-element.100.refs_4_), channel_id=1, source_target_pairs={{0,3},{1,2},{2,1},{3,0},{4,7},{5,6},{6,5},{7,4},{8,11},{9,10},{10,... | collective-permute-start | bytes 786440 | tf_op jit(solution)/shard_map/ppermute | solution.py:19
  197.1 16.3 %collective-permute-start.36 = (bf16[1024,128]{1,0:T(8,128)(2,1)S(1)}, bf16[1024,128]{1,0:T(8,128)(2,1)S(1)}, u32[]{:S(2)}, u32[]{:S(2)}) collective-permute-start(bf16[1024,128]{1,0:T(8,128)(2,1)S(1)} %get-tuple-element.97.refs_0_), channel_id=1, source_target_pairs={{0,2},{1,3},{2,0},{3,1},{4,6},{5,7},{6,4},{7,5},{8,10},{9,11},{10,... | collective-permute-start | bytes 786440 | tf_op jit(solution)/shard_map/ppermute | solution.py:19
  197.7 15.7 %collective-permute-start.37 = (bf16[1024,128]{1,0:T(8,128)(2,1)S(1)}, bf16[1024,128]{1,0:T(8,128)(2,1)S(1)}, u32[]{:S(2)}, u32[]{:S(2)}) collective-permute-start(bf16[1024,128]{1,0:T(8,128)(2,1)S(1)} %get-tuple-element.97.refs_0_), channel_id=1, source_target_pairs={{0,3},{1,2},{2,1},{3,0},{4,7},{5,6},{6,5},{7,4},{8,11},{9,10},{10,... | collective-permute-start | bytes 786440 | tf_op jit(solution)/shard_map/ppermute | solution.py:19
  199.4 14.1 %collective-permute-start.38 = (bf16[1024,128]{1,0:T(8,128)(2,1)}, bf16[1024,128]{1,0:T(8,128)(2,1)S(1)}, u32[]{:S(2)}, u32[]{:S(2)}) collective-permute-start(bf16[1024,128]{1,0:T(8,128)(2,1)} %get-tuple-element.98.refs_4_), channel_id=1, source_target_pairs={{0,1},{1,0},{2,3},{3,2},{4,5},{5,4},{6,7},{7,6},{8,9},{9,8},{10,11... | collective-permute-start | bytes 786440 | tf_op jit(solution)/shard_map/ppermute | solution.py:19
  200.7 23.1 %collective-permute-start.39 = (bf16[1024,128]{1,0:T(8,128)(2,1)}, bf16[1024,128]{1,0:T(8,128)(2,1)S(1)}, u32[]{:S(2)}, u32[]{:S(2)}) collective-permute-start(bf16[1024,128]{1,0:T(8,128)(2,1)} %get-tuple-element.98.refs_4_), channel_id=1, source_target_pairs={{0,2},{1,3},{2,0},{3,1},{4,6},{5,7},{6,4},{7,5},{8,10},{9,11},{10,... | collective-permute-start | bytes 786440 | tf_op jit(solution)/shard_map/ppermute | solution.py:19
  201.3 22.5 %collective-permute-start.40 = (bf16[1024,128]{1,0:T(8,128)(2,1)}, bf16[1024,128]{1,0:T(8,128)(2,1)}, u32[]{:S(2)}, u32[]{:S(2)}) collective-permute-start(bf16[1024,128]{1,0:T(8,128)(2,1)} %get-tuple-element.98.refs_4_), channel_id=1, source_target_pairs={{0,3},{1,2},{2,1},{3,0},{4,7},{5,6},{6,5},{7,4},{8,11},{9,10},{10,... | collective-permute-start | bytes 786440 | tf_op jit(solution)/shard_map/ppermute | solution.py:19
  230.1 18.9 %collective-permute-start.56 = (bf16[128,512]{1,0:T(8,128)(2,1)S(1)}, bf16[128,512]{1,0:T(8,128)(2,1)S(1)}, u32[]{:S(2)}, u32[]{:S(2)}) collective-permute-start(bf16[128,512]{1,0:T(8,128)(2,1)S(1)} %get-tuple-element.109), channel_id=1, source_target_pairs={{0,16},{4,20},{8,24},{12,28},{16,0},{20,4},{24,8},{28,12},{1,17},{... | collective-permute-start | bytes 393224 | tf_op jit(solution)/shard_map/ppermute | solution.py:19
  (98 other events, 482.7 us)
